TPU v7x, 256 devices: a whole 4x4x8 slice. The times are simulated.
256 devices in a mesh: sp: 16 (over y, x), tp: 16 (over z, core).
Axes of the slice: x: 4, y: 4, z: 8, core: 2. Of those that a mesh axis runs over, the one named last changes fastest.
Arguments:
- linear_part: bfloat16 [32768, 2048], P('sp', 'tp'), may hold values from -6 to 6
- gate_part: bfloat16 [32768, 2048], P('sp', 'tp'), may hold values from -8 to 8
- kernel_taps: bfloat16 [31, 2048], P(None, 'tp'), may hold values from -10 to 10
- channel_gain: float32 [2048], replicated, may hold values from 0.1 to 1.9
- output_weight: bfloat16 [2048, 2048], P('tp'), may hold values from -0.125 to 0.125
- residual: bfloat16 [32768, 2048], P(('sp', 'tp')), may hold values from -6 to 6
- mix_gain: float32 [2048], replicated, may hold values from 0.1 to 1.9
- documents: int32 [32768], P('sp'), may hold values from 0 to 3, never falling along the last dimension, each value on 1 to 16384 neighbouring positions
- expert_ids: int32 [32768, 2], P(('sp', 'tp')), may hold values from 0 to 15, all different within a row; in each aligned block of 128 rows (0 to 127, 128 to 255, ...) at most 64 rows name the same one
- route_weights: float32 [32768, 2], P(('sp', 'tp')), may hold values from 0.25 to 2.5
- expert_gate: bfloat16 [16, 2048, 512], P('sp'), may hold values from -0.125 to 0.125
- expert_up: bfloat16 [16, 2048, 512], P('sp'), may hold values from -0.125 to 0.125
- expert_down: bfloat16 [16, 512, 2048], P('sp'), may hold values from -0.25 to 0.25
- shared_gate: bfloat16 [2048, 256], replicated, may hold values from -0.125 to 0.125
- shared_up: bfloat16 [2048, 256], replicated, may hold values from -0.125 to 0.125
- shared_down: bfloat16 [256, 2048], replicated, may hold values from -0.375 to 0.375
- final_gain: float32 [2048], replicated, may hold values from 0.1 to 1.9
Outputs:
- layer_out: bfloat16 [32768, 2048], P(('sp', 'tp'))
Inputs may be any that keep to these rules, and one draw needn't show every extreme that they name: `expert_ids`: each row names 2 different experts; among the rows of one device (aligned blocks of 128 rows) no expert is named by more than 64 rows, and exactly 64 in some block. `documents`: never falling along the sequence; each document 1 to 16384 positions.
All inputs are finite; a program needn't handle non-finite values.
Results may differ from a plain program's by a relative error of at most 0.0065.
Values may be sent and summed in bfloat16 or wider, within the bound.
A program may use at most 64 MiB of HBM per device.

v0:
```python
import jax
import jax.numpy as jnp
from jax import lax
from jax.sharding import Mesh
from jax.sharding import PartitionSpec as P

TP = ("tp_0", "tp_1")
SP_TP = ("sp", "tp_0", "tp_1")


EPSILON = 1e-05
RESIDUAL_SCALE = 8.0**0.25


def passed_along(block, axis, distance):
    devices = range(lax.axis_size(axis))
    route = [(i - distance, i) for i in devices if i - distance in devices]
    return lax.ppermute(block, axis, route)


def cut_along(x, dim, length):
    before, after = (x.shape[:dim], x.shape[dim + 1 :])
    return jnp.moveaxis(x.reshape(*before, length, -1, *after), dim, 0)


def laid_out(tiles, dim):
    lengths = list(tiles.shape[1:])
    lengths[dim] *= tiles.shape[0]
    return jnp.moveaxis(tiles, 0, dim).reshape(lengths)


def exchange_in_order(tiles, axes, turns):
    inside = tiles.shape[1:]
    whole = tiles.reshape(*(lax.axis_size(a) for a in axes), *inside)
    for k in turns:
        whole = lax.all_to_all(whole, axes[k], k, k, tiled=True)
    return whole.reshape(-1, *inside)


def exchange_by_axis(x, axes, turns, split_dim, concat_dim):
    tiles = cut_along(x, split_dim, lax.axis_size(axes))
    return laid_out(exchange_in_order(tiles, axes, turns), concat_dim)


def normalize(values):
    mean = jnp.mean(values, -1, keepdims=True)
    square = jnp.mean(values * values, -1, keepdims=True)
    return (values - mean) * lax.rsqrt(square - mean * mean + EPSILON)


def shards(
    linear_part,
    gate_part,
    kernel_taps,
    channel_gain,
    output_weight,
    residual,
    mix_gain,
    documents,
    expert_ids,
    route_weights,
    expert_gate,
    expert_up,
    expert_down,
    shared_gate,
    shared_up,
    shared_down,
    final_gain,
):
    reach = kernel_taps.shape[0] - 1
    length = linear_part.shape[0]
    gated = (
        linear_part.astype(jnp.float32) * jax.nn.sigmoid(gate_part.astype(jnp.float32))
    ).astype(jnp.bfloat16)
    before, before_docs = passed_along(
        (gated[length - reach :], documents[length - reach :]), "sp", 1
    )
    extended = jnp.concatenate([before, gated], 0)
    extended_docs = jnp.concatenate([before_docs, documents], 0)
    taps = kernel_taps.astype(jnp.float32)
    total = jnp.zeros(gated.shape, jnp.float32)
    for offset in range(reach + 1):
        window = lax.slice_in_dim(extended, reach - offset, reach - offset + length, axis=0).astype(
            jnp.float32
        )
        same = (
            lax.slice_in_dim(extended_docs, reach - offset, reach - offset + length, axis=0)
            == documents
        )
        total = total + jnp.where(same[:, None], window * taps[offset], 0.0)
    convolved = total.astype(jnp.bfloat16)
    position_rows = exchange_by_axis(convolved, TP, (1, 0), 0, 1)
    activated = jax.nn.silu(normalize(position_rows.astype(jnp.float32)) * channel_gain).astype(
        jnp.bfloat16
    )
    full_weight = lax.all_gather(output_weight, TP, axis=0, tiled=True)
    projected = jnp.dot(activated, full_weight, preferred_element_type=jnp.float32)
    normed = (
        normalize(RESIDUAL_SCALE * residual.astype(jnp.float32) + projected) * mix_gain
    ).astype(jnp.bfloat16)
    rows = normed.shape[0]
    width_full = normed.shape[1]
    chosen = expert_ids.shape[1]
    experts_all = lax.axis_size("sp") * expert_gate.shape[0]
    capacity = min(rows, 4 * rows * chosen // experts_all)
    flat_ids = expert_ids.reshape(-1)
    onehot = (flat_ids[:, None] == jnp.arange(experts_all, dtype=jnp.int32)[None, :]).astype(
        jnp.int32
    )
    earlier = jnp.cumsum(onehot, 0) - onehot
    ranks = jnp.sum(earlier * onehot, 1)
    slots = flat_ids * capacity + ranks
    places = jnp.arange(experts_all * capacity, dtype=jnp.int32)[:, None] == slots[None, :]
    chooser = jnp.any(places.reshape(experts_all * capacity, rows, chosen), 2).astype(jnp.bfloat16)
    outgoing = jnp.dot(chooser, normed, preferred_element_type=jnp.float32).astype(jnp.bfloat16)
    outgoing = outgoing.reshape(experts_all, capacity, width_full)
    arrived = lax.all_to_all(outgoing, "sp", split_axis=0, concat_axis=0, tiled=True)
    sources, items, width = arrived.shape
    flat = arrived.reshape(sources * items, width)
    hidden = (
        jax.nn.silu(jnp.dot(flat, expert_gate[0], preferred_element_type=jnp.float32))
        * jnp.dot(flat, expert_up[0], preferred_element_type=jnp.float32)
    ).astype(jnp.bfloat16)
    answer = jnp.dot(hidden, expert_down[0], preferred_element_type=jnp.float32).astype(
        jnp.bfloat16
    )
    answered = answer.reshape(sources, items, width)
    returned = lax.all_to_all(answered, "sp", split_axis=0, concat_axis=0, tiled=True).reshape(
        experts_all * capacity, width_full
    )
    picked = jnp.take(returned, slots, axis=0).astype(jnp.float32).reshape(rows, chosen, width_full)
    routed = jnp.sum(picked * route_weights[:, :, None], 1)
    common = (
        jax.nn.silu(jnp.dot(normed, shared_gate, preferred_element_type=jnp.float32))
        * jnp.dot(normed, shared_up, preferred_element_type=jnp.float32)
    ).astype(jnp.bfloat16)
    shared_out = jnp.dot(common, shared_down, preferred_element_type=jnp.float32)
    return (
        normalize(RESIDUAL_SCALE * normed.astype(jnp.float32) + routed + shared_out) * final_gain
    ).astype(jnp.bfloat16)


def solution(mesh):
    finer = Mesh(mesh.devices.reshape(mesh.shape["sp"], 8, 2), ("sp", "tp_0", "tp_1"))
    placed = (
        P("sp", TP),
        P("sp", TP),
        P(None, TP),
        P(),
        P(TP, None),
        P(SP_TP, None),
        P(),
        P("sp"),
        P(SP_TP, None),
        P(SP_TP, None),
        P("sp", None, None),
        P("sp", None, None),
        P("sp", None, None),
        P(),
        P(),
        P(),
        P(),
    )
    return jax.shard_map(
        shards, mesh=finer, in_specs=placed, out_specs=P(SP_TP, None), check_vma=False
    )
```

profile of v0, /device:TPU:1, one launch (start us, length us, event | category | flops | bytes accessed | tf_op | source)
XLA Modules:
  0.0 252.0 jit_solution(5865854858807349603)
XLA Ops:
  6.5 0.0 copy-start
  6.5 0.0 copy-start.2
  6.5 0.0 all-gather.2.cloned.1.call-start
  6.5 0.7 all-gather.2.cloned.1.call-update
  7.3 0.8 slice.286
  8.0 3.9 %collective-permute-start = (s32[30]{0:T(128)S(1)}, s32[30]{0:T(128)S(1)}, u32[]{:S(2)}, u32[]{:S(2)}) collective-permute-start(s32[30]{0:T(128)S(1)} %slice.286), channel_id=1, source_target_pairs={{0,16},{16,32},{32,48},{48,64},{64,80},{80,96},{96,112},{112,128},... | collective-permute-start | bytes 368 | tf_op jit(solution)/shard_map/ppermute | solution.py:18
  12.0 1.5 multiply_convert_fusion.4
  13.5 3.1 %collective-permute-start.1 = (bf16[30,128]{1,0:T(8,128)(2,1)S(1)}, bf16[30,128]{1,0:T(8,128)(2,1)S(1)}, u32[]{:S(2)}, u32[]{:S(2)}) collective-permute-start(bf16[30,128]{1,0:T(8,128)(2,1)S(1)} %slice.385), channel_id=1, source_target_pairs={{0,16},{16,32},{32,48},{48,64},{64,80},{80,96},{96,112},{112,128},... | collective-permute-start | bytes 23048 | tf_op jit(solution)/shard_map/ppermute | solution.py:18
  16.6 0.0 copy-done.7
  16.6 0.0 collective-permute-done
  16.6 0.0 copy-done.2
  16.7 0.1 fusion.55
  16.8 0.1 fusion.57
  16.9 0.1 fusion.59
  17.0 0.1 fusion.109
  17.1 0.3 collective-permute-done.1
  17.4 11.1 %add_convert_fusion = bf16[2048,128]{1,0:T(8,128)(2,1)S(1)} fusion(bf16[2048,128]{1,0:T(8,128)(2,1)S(1)} %multiply_convert_fusion.4, bf16[30,128]{1,0:T(8,128)(2,1)S(1)} %collective-permute-done.1, f32[128]{0:T(128)S(1)} %get-tuple-element.14, f32[128]{0:T(128)S(1)} %get-tuple-element.15, f32[128]{0:T(128)S(1)} %get-tuple-element.16, ...), kind=kLoop, calls=%fused_computation.54 | loop fusion | flops 55836672 | bytes 1133568 | tf_op jit(solution)/shard_map/convert_element_type | solution.py:91
  28.5 0.0 copy-start.3
  28.5 0.3 copy.55
  28.8 0.0 copy-start.4
  28.8 5.6 %all_to_all.20 = bf16[8,2,128,128]{2,3,0,1:T(8,128)(2,1)S(1)} all-to-all(bf16[8,2,128,128]{2,3,0,1:T(8,128)(2,1)S(1)} %copy.55), channel_id=1, replica_groups=mesh['sp'=16,'tp_0'=8,'tp_1'=2] {'tp_1'}, dimensions={1} | all-to-all | bytes 1048576 | tf_op jit(solution)/shard_map/all_to_all | solution.py:36
  34.4 0.8 copy.56
  35.2 8.4 %all-to-all-start.1 = ((bf16[8,2,128,128]{2,3,1,0:T(8,128)(2,1)}), bf16[8,2,128,128]{2,3,1,0:T(8,128)(2,1)S(1)}, u32[]{:S(2)}, u32[]{:S(2)}) async-start(bf16[8,2,128,128]{2,3,1,0:T(8,128)(2,1)} %copy.56), calls=%async_computation.1 | async-start | bytes 1048576 | tf_op jit(solution)/shard_map/all_to_all | solution.py:36
  43.6 0.0 copy-done.3
  43.6 0.1 copy.57
  43.7 0.1 eq.160
  43.9 0.1 reshape.187
  44.0 0.6 reduce-window.6
  44.6 0.2 slice_reduce_fusion
  44.8 0.1 fusion.50
  44.9 0.1 reduce_sum.81
  45.1 0.1 copy.60
  45.2 0.1 fusion.10
  45.3 21.7 %all-to-all-done.1 = bf16[8,2,128,128]{2,3,1,0:T(8,128)(2,1)S(1)} async-done(((bf16[8,2,128,128]{2,3,1,0:T(8,128)(2,1)}), bf16[8,2,128,128]{2,3,1,0:T(8,128)(2,1)S(1)}, u32[]{:S(2)}, u32[]{:S(2)}) %all-to-all-start.1) | async-done | bytes 524320 | tf_op jit(solution)/shard_map/all_to_all | solution.py:36
  67.0 0.3 convert_reduce_fusion
  67.3 0.0 copy-done.4
  67.3 0.4 multiply_convert_fusion.3
  67.7 0.0 copy-start.5
  67.7 12.7 %all-gather.2.cloned.1.call-done = bf16[2048,2048]{1,0:T(8,128)(2,1)} async-done(((bf16[128,2048]{1,0:T(8,128)(2,1)}), bf16[2048,2048]{1,0:T(8,128)(2,1)}) %all-gather.2.cloned.1.call-update) | async-done | bytes 8388624 | tf_op jit(solution)/shard_map/all_gather | solution.py:96
  80.5 4.8 %fusion.115 = (f32[128]{0:T(128)S(1)}, f32[128]{0:T(128)S(1)}, f32[128,2048]{1,0:T(8,128)S(1)}) fusion(bf16[128,2048]{0,1:T(8,128)(2,1)S(1)} %multiply_convert_fusion.3, bf16[2048,2048]{1,0:T(8,128)(2,1)} %all-gather.2.cloned.1.call-done, bf16[128,2048]{1,0:T(8,128)(2,1)} %param.22), kind=kOutput, calls=%fused_computation.271 | convolution fusion | flops 1075314432 | bytes 10486784 | tf_op jit(solution)/shard_map/dot_general | solution.py:97
  85.3 0.0 copy-done.5
  85.3 0.2 multiply_convert_fusion.2
  85.5 1.2 convolution_convert_fusion.1
  86.8 0.0 copy-start.9
  86.8 56.6 %all_to_all.21 = bf16[16,64,2048]{2,1,0:T(8,128)(2,1)S(1)} all-to-all(bf16[16,64,2048]{2,1,0:T(8,128)(2,1)S(1)} %bitcast.124), channel_id=1, replica_groups=mesh['sp'=16,'tp_0'=8,'tp_1'=2] {'sp'}, dimensions={0} | all-to-all | bytes 8388608 | tf_op jit(solution)/shard_map/all_to_all | solution.py:117
  143.4 2.0 copy-done.1
  145.4 0.0 copy-done.9
  145.4 3.8 %fusion.1 = f32[1024,512]{1,0:T(8,128)} fusion(bf16[1024,2048]{1,0:T(8,128)(2,1)S(1)} %bitcast.126, bf16[1,2048,512]{2,1,0:T(8,128)(2,1)S(1)} %copy-done.9), kind=kOutput, calls=%fused_computation.35 | convolution fusion | flops 2147483648 | bytes 8388608 | tf_op jit(solution)/shard_map/dot_general | solution.py:122
  149.1 0.0 copy-done
  149.1 10.0 %convolution_convert_fusion = bf16[1024,2048]{1,0:T(8,128)(2,1)} fusion(bf16[1,512,2048]{2,1,0:T(8,128)(2,1)S(1)} %copy-done, f32[1024,512]{1,0:T(8,128)} %fusion.1, bf16[1024,2048]{1,0:T(8,128)(2,1)} %bitcast.127, bf16[1,2048,512]{2,1,0:T(8,128)(2,1)} %param.27), kind=kOutput, calls=%fused_computation.30 | convolution fusion | flops 4300210176 | bytes 14680064 | tf_op jit(solution)/shard_map/dot_general | solution.py:124
  159.2 4.7 %all-to-all-start.3 = ((bf16[16,64,2048]{2,1,0:T(8,128)(2,1)}), bf16[16,64,2048]{2,1,0:T(8,128)(2,1)}, u32[]{:S(2)}, u32[]{:S(2)}) async-start(bf16[16,64,2048]{2,1,0:T(8,128)(2,1)} %bitcast.125), calls=%async_computation.3 | async-start | bytes 8388608 | tf_op jit(solution)/shard_map/all_to_all | solution.py:128
  163.9 0.1 copy.62
  164.0 0.1 mul.569
  164.1 0.1 copy.61
  164.3 0.0 copy-done.8
  164.3 0.1 copy.63
  164.4 1.5 fusion.117
  165.9 58.3 %all-to-all-done.3 = bf16[16,64,2048]{2,1,0:T(8,128)(2,1)} async-done(((bf16[16,64,2048]{2,1,0:T(8,128)(2,1)}), bf16[16,64,2048]{2,1,0:T(8,128)(2,1)}, u32[]{:S(2)}, u32[]{:S(2)}) %all-to-all-start.3) | async-done | bytes 4194336 | tf_op jit(solution)/shard_map/all_to_all | solution.py:128
  224.2 6.1 %gather_fusion = bf16[256,2048]{1,0:T(8,128)(2,1)} fusion(bf16[1024,2048]{1,0:T(8,128)(2,1)} %bitcast.42, s32[1024]{0:T(1024)S(1)} %pad_clamp_fusion), kind=kCustom, calls=%fused_computation | custom fusion | bytes 2098176 | tf_op jit(solution)/shard_map/jit(_take)/gather | solution.py:131
  230.3 2.5 %gather.7 = bf16[128,2,2048]{2,1,0:T(2,128)(2,1)} reshape(bf16[256,2048]{1,0:T(8,128)(2,1)} %gather_fusion) | data formatting | bytes 2097152 | tf_op jit(solution)/shard_map/jit(_take)/gather | solution.py:131
  232.9 6.4 %multiply_reduce_fusion = f32[128,2048]{1,0:T(8,128)} fusion(bf16[128,2,2048]{2,1,0:T(2,128)(2,1)} %gather.7, pred[128,2]{1,0:T(8,128)(4,1)S(1)} %copy.61, f32[128,2]{1,0:T(8,128)S(1)} %copy.63), kind=kLoop, calls=%fused_computation.39 | loop fusion | flops 1835008 | bytes 2098432 | tf_op jit(solution)/shard_map/reduce_sum | solution.py:132
  239.3 3.6 %fusion.114 = (f32[128]{0:T(128)S(1)}, f32[128]{0:T(128)S(1)}, f32[128,2048]{1,0:T(8,128)}) fusion(bf16[256,2048]{1,0:T(8,128)(2,1)} %param.32, bf16[128,2048]{1,0:T(8,128)(2,1)S(1)} %multiply_convert_fusion.2, bf16[2048,256]{1,0:T(8,128)(2,1)} %param.31, f32[128,256]{1,0:T(8,128)S(1)} %fusion.117, f32[128,2048]{1,0:T(8,128)} %multiply_reduce_fusion), kind=kOutput, calls=%fused_computation.270 | convolution fusion | flops 270466816 | bytes 4850688 | tf_op jit(solution)/shard_map/dot_general | solution.py:137
  242.9 0.0 copy-done.6
  242.9 2.2 multiply_convert_fusion.1
  (18 shorter events, 0.2 us)
Async XLA Ops:
  6.5 142.6 %copy-start = (bf16[1,512,2048]{2,1,0:T(8,128)(2,1)S(1)}, bf16[1,512,2048]{2,1,0:T(8,128)(2,1)}, u32[]{:S(2)}) copy-start(bf16[1,512,2048]{2,1,0:T(8,128)(2,1)} %param.29) | copy-start | bytes 6291460
  6.5 10.1 %copy-start.2 = (s32[2048]{0:T(1024)S(1)}, s32[2048]{0:T(1024)}, u32[]{:S(2)}) copy-start(s32[2048]{0:T(1024)} %param.24) | copy-start | bytes 24580
  6.5 10.0 %copy-start.7 = (bf16[31,128]{1,0:T(8,128)(2,1)S(1)}, bf16[31,128]{1,0:T(8,128)(2,1)}, u32[]{:S(2)}) copy-start(bf16[31,128]{1,0:T(8,128)(2,1)} %param.19) | copy-start | bytes 23812
  6.5 73.9 %all-gather.2.cloned.1.call-start = ((), (), s32[]{:S(2)}) async-start(), calls=%async_computation.4 | async-start | bytes 8912896 | tf_op jit(solution)/shard_map/all_gather | solution.py:96
  8.0 8.6 %collective-permute-start = (s32[30]{0:T(128)S(1)}, s32[30]{0:T(128)S(1)}, u32[]{:S(2)}, u32[]{:S(2)}) collective-permute-start(s32[30]{0:T(128)S(1)} %slice.286), channel_id=1, source_target_pairs={{0,16},{16,32},{32,48},{48,64},{64,80},{80,96},{96,112},{112,128},... | collective-permute-start | bytes 368 | tf_op jit(solution)/shard_map/ppermute | solution.py:18
  13.5 3.9 %collective-permute-start.1 = (bf16[30,128]{1,0:T(8,128)(2,1)S(1)}, bf16[30,128]{1,0:T(8,128)(2,1)S(1)}, u32[]{:S(2)}, u32[]{:S(2)}) collective-permute-start(bf16[30,128]{1,0:T(8,128)(2,1)S(1)} %slice.385), channel_id=1, source_target_pairs={{0,16},{16,32},{32,48},{48,64},{64,80},{80,96},{96,112},{112,128},... | collective-permute-start | bytes 23048 | tf_op jit(solution)/shard_map/ppermute | solution.py:18
  28.5 15.1 %copy-start.3 = (s32[128,2]{0,1:T(2,128)S(1)}, s32[128,2]{0,1:T(2,128)}, u32[]{:S(2)}) copy-start(s32[128,2]{0,1:T(2,128)} %param.25) | copy-start | bytes 3076
  28.8 38.6 %copy-start.4 = (f32[2048]{0:T(1024)S(1)}, f32[2048]{0:T(1024)}, u32[]{:S(2)}) copy-start(f32[2048]{0:T(1024)} %param.20) | copy-start | bytes 24580
  35.2 31.8 %all-to-all-start.1 = ((bf16[8,2,128,128]{2,3,1,0:T(8,128)(2,1)}), bf16[8,2,128,128]{2,3,1,0:T(8,128)(2,1)S(1)}, u32[]{:S(2)}, u32[]{:S(2)}) async-start(bf16[8,2,128,128]{2,3,1,0:T(8,128)(2,1)} %copy.56), calls=%async_computation.1 | async-start | bytes 1048576 | tf_op jit(solution)/shard_map/all_to_all | solution.py:36
  67.7 17.6 %copy-start.5 = (f32[2048]{0:T(1024)S(1)}, f32[2048]{0:T(1024)}, u32[]{:S(2)}) copy-start(f32[2048]{0:T(1024)} %param.23) | copy-start | bytes 24580
  86.8 58.6 %copy-start.9 = (bf16[1,2048,512]{2,1,0:T(8,128)(2,1)S(1)}, bf16[1,2048,512]{2,1,0:T(8,128)(2,1)}, u32[]{:S(2)}) copy-start(bf16[1,2048,512]{2,1,0:T(8,128)(2,1)} %param.28) | copy-start | bytes 6291460
  143.4 2.0 copy-start.1
  159.2 5.1 %copy-start.8 = (f32[128,2]{0,1:T(2,128)S(1)}, f32[128,2]{0,1:T(2,128)}, u32[]{:S(2)}) copy-start(f32[128,2]{0,1:T(2,128)} %param.26) | copy-start | bytes 3076
  159.2 65.1 %all-to-all-start.3 = ((bf16[16,64,2048]{2,1,0:T(8,128)(2,1)}), bf16[16,64,2048]{2,1,0:T(8,128)(2,1)}, u32[]{:S(2)}, u32[]{:S(2)}) async-start(bf16[16,64,2048]{2,1,0:T(8,128)(2,1)} %bitcast.125), calls=%async_computation.3 | async-start | bytes 8388608 | tf_op jit(solution)/shard_map/all_to_all | solution.py:128
  239.3 3.7 %copy-start.6 = (f32[2048]{0:T(1024)S(1)}, f32[2048]{0:T(1024)}, u32[]{:S(2)}) copy-start(f32[2048]{0:T(1024)} %param.33) | copy-start | bytes 24580
Sparse Core Ops, SparseCore 0:
  9.2 71.2 all-gather.1
where the time goes:
time: 253 us; the launch traced here: 252 us
  waiting for transfers between devices  93.8 us (37%)
  blocking collectives  62.2 us (25%)
  matrix products  25 us (10%)
  other arithmetic  23.4 us (9%)
  starting transfers between devices  20.1 us (8%)
  local copies, waits for them, and re-layouts  13.8 us (5%)
  between operations  13.7 us (5%)
    all_to_all x1, waiting for transfers between devices, shards(): lax.all_to_all(answered, 'sp', split_axis=0, concat_axis=0, tiled=True)  58.3 us
    all_to_all x1, blocking collectives, shards(): lax.all_to_all(outgoing, 'sp', split_axis=0, concat_axis=0, tiled=True)  56.6 us
    all_to_all x1, waiting for transfers between devices, exchange_in_order(): whole = lax.all_to_all(whole, axes[k], k, k, tiled=True)  21.7 us
    all_gather x1, waiting for transfers between devices, shards(): full_weight = lax.all_gather(output_weight, TP, axis=0, tiled=True)  12.7 us
    convert_element_type x1, other arithmetic, shards(): convolved = total.astype(jnp.bfloat16)  11.1 us
    dot_general x1, matrix products, shards(): jnp.dot(hidden, expert_down[0], preferred_element_type=jnp.float32)  10 us
    gather x2, local copies, waits for them, and re-layouts, shards(): jnp.take(returned, slots, axis=0).astype(jnp.float32)  8.62 us
    all_to_all x1, starting transfers between devices, exchange_in_order(): whole = lax.all_to_all(whole, axes[k], k, k, tiled=True)  8.41 us
  transfers between devices with their start and end apart: 5, of which 4 were waited for; matrix products, arithmetic and copies ran while one was open for 8% of the time, Pallas kernels for 0%

commit v1 on v0

--- a/solution.py
+++ b/solution.py
@@ -1,6 +1,8 @@
 import jax
 import jax.numpy as jnp
 from jax import lax
+from jax.experimental import pallas as pl
+from jax.experimental.pallas import tpu as pltpu
 from jax.sharding import Mesh
 from jax.sharding import PartitionSpec as P
 
@@ -46,6 +48,299 @@
     mean = jnp.mean(values, -1, keepdims=True)
     square = jnp.mean(values * values, -1, keepdims=True)
     return (values - mean) * lax.rsqrt(square - mean * mean + EPSILON)
+
+
+MESH_ID = pl.DeviceIdType.MESH
+HALF = 1024
+SIDE = 4
+CAP = 64
+
+
+def expert_kernel(
+    normed, table, gain, w_gate, w_up, w_down, s_gate, s_up, s_down, out,
+    wg, wu, wd, sg, su, sd,
+    near, meta, packed, relay, arrived, acc_g, acc_u, answers, relay_back, back, partial, relay_part, part_in,
+    kept, shared,
+    w_sem, s1_s, s1_r, m_s, m_r, d_s, d_r, rl_s, rl_r, fw_s, fw_r,
+    b_s, b_r, bl_s, bl_r, bf_s, bf_r, p_s, p_r,
+):
+    f32, bf16 = jnp.float32, jnp.bfloat16
+    sp, tp = lax.axis_index("sp"), (lax.axis_index("tp_0"), lax.axis_index("tp_1"))
+    y, x = sp // SIDE, sp % SIDE
+
+    def at(dy, dx):
+        return ((y + dy) % SIDE) * SIDE + (x + dx) % SIDE
+
+    def first(o, k):
+        return at(0, k) if o == 0 else at(k, 0)
+
+    def second(o, k):
+        return at(k, 0) if o == 0 else at(0, k)
+
+    def send(src, dst, ss, rs, to):
+        copy = pltpu.make_async_remote_copy(
+            src_ref=src, dst_ref=dst, send_sem=ss, recv_sem=rs,
+            device_id=(to, *tp), device_id_type=MESH_ID,
+        )
+        copy.start()
+        sent.append(copy)
+
+    def landed(dst, ss, rs):
+        pltpu.make_async_remote_copy(
+            src_ref=dst, dst_ref=dst, send_sem=ss, recv_sem=rs,
+            device_id=(first(0, 1), *tp), device_id_type=MESH_ID,
+        ).wait_recv()
+
+    sent = []
+    loads = [
+        pltpu.make_async_copy(a, b, w_sem.at[i])
+        for i, (a, b) in enumerate(
+            [(s_gate, sg), (s_up, su), (s_down, sd), (w_gate, wg), (w_up, wu), (w_down, wd)]
+        )
+    ]
+    for load in loads:
+        load.start()
+
+    barrier = pltpu.get_barrier_semaphore()
+    for to in (at(0, 1), at(0, 3), at(1, 0), at(3, 0)):
+        pl.semaphore_signal(barrier, inc=1, device_id=(to, *tp), device_id_type=MESH_ID)
+    pl.semaphore_wait(barrier, 4)
+
+    for o in (0, 1):
+        mine = normed.at[:, o * HALF:(o + 1) * HALF]
+        send(table, meta.at[o, 3], m_s.at[o, 0], m_r.at[o, 0], first(o, 1))
+        send(table, meta.at[o, 1], m_s.at[o, 1], m_r.at[o, 1], first(o, 3))
+        send(mine, near.at[o, 3], s1_s.at[o, 0], s1_r.at[o, 0], first(o, 1))
+        send(mine, near.at[o, 1], s1_s.at[o, 1], s1_r.at[o, 1], first(o, 3))
+
+    lanes = lax.broadcasted_iota(jnp.int32, (CAP, 128), 0).astype(f32)
+
+    def expert_at(o, k):
+        return second(o, k)
+
+    def slot_row(o, k, e):
+        return table[e] if k == 0 else meta[o, k, e]
+
+    def weight_row(o, k, e):
+        return table[e + 16] if k == 0 else meta[o, k, e + 16]
+
+    def pack(o, k):
+        rows = normed[:, o * HALF:(o + 1) * HALF] if k == 0 else near[o, k]
+        for q in (2, 1, 3, 0):
+            hit = jnp.where(lanes == slot_row(o, k, expert_at(o, q)), 1.0, 0.0).astype(bf16)
+            block = jnp.dot(hit, rows, preferred_element_type=f32).astype(bf16)
+            if q == 0:
+                arrived[o, 0, k] = block
+            else:
+                packed[o, q - 1, k] = block
+            if q == 2:
+                way = 1 if k < 2 else 3
+                send(packed.at[o, 1, k], relay.at[o, k], rl_s.at[o, k], rl_r.at[o, k], second(o, way))
+            if q == 1:
+                send(packed.at[o, 0, k], arrived.at[o, 3, k], d_s.at[o, 0, k], d_r.at[o, 0, k], second(o, 1))
+            if q == 3:
+                send(packed.at[o, 2, k], arrived.at[o, 1, k], d_s.at[o, 1, k], d_r.at[o, 1, k], second(o, 3))
+
+    def pass_on(o, k):
+        landed(relay.at[o, k], rl_s.at[o, k], rl_r.at[o, k])
+        way = 1 if k < 2 else 3
+        send(relay.at[o, k], arrived.at[o, 2, k], fw_s.at[o, k], fw_r.at[o, k], second(o, way))
+
+    for o in (0, 1):
+        pack(o, 0)
+    for o in (0, 1):
+        landed(meta.at[o, 3], m_s.at[o, 0], m_r.at[o, 0])
+        send(meta.at[o, 3], meta.at[o, 2], m_s.at[o, 2], m_r.at[o, 2], first(o, 1))
+        landed(near.at[o, 3], s1_s.at[o, 0], s1_r.at[o, 0])
+        send(near.at[o, 3, 0:64], near.at[o, 2, 0:64], s1_s.at[o, 2], s1_r.at[o, 2], first(o, 1))
+    for o in (0, 1):
+        landed(meta.at[o, 1], m_s.at[o, 1], m_r.at[o, 1])
+        landed(near.at[o, 1], s1_s.at[o, 1], s1_r.at[o, 1])
+        send(near.at[o, 1, 64:128], near.at[o, 2, 64:128], s1_s.at[o, 3], s1_r.at[o, 3], first(o, 3))
+    for k in (3, 1):
+        for o in (0, 1):
+            pack(o, k)
+    for o in (0, 1):
+        pass_on(o, 0)
+    for o in (0, 1):
+        landed(meta.at[o, 2], m_s.at[o, 2], m_r.at[o, 2])
+        landed(near.at[o, 2, 0:64], s1_s.at[o, 2], s1_r.at[o, 2])
+        landed(near.at[o, 2, 64:128], s1_s.at[o, 3], s1_r.at[o, 3])
+        pack(o, 2)
+
+    for load in loads[:3]:
+        load.wait()
+    act = jnp.dot(normed[...], sg[...], preferred_element_type=f32)
+    lin = jnp.dot(normed[...], su[...], preferred_element_type=f32)
+    common = (act / (1.0 + jnp.exp(-act)) * lin).astype(bf16)
+    shared[...] = jnp.dot(common, sd[...], preferred_element_type=f32)
+    for k in (3, 1, 2):
+        for o in (0, 1):
+            pass_on(o, k)
+    for load in loads[3:]:
+        load.wait()
+
+    def product(o, q):
+        rows = arrived[o, q].reshape(SIDE * CAP, HALF)
+        for acc, w in ((acc_g, wg), (acc_u, wu)):
+            got = jnp.dot(rows, w[o * HALF:(o + 1) * HALF, :], preferred_element_type=f32)
+            got = got.reshape(SIDE, CAP, 512)
+            if o == 0:
+                acc[q] = got
+            else:
+                acc[:, q] = acc[:, q] + got
+
+    def from_side(q, d):
+        for k in range(SIDE):
+            for o in (0, 1):
+                landed(arrived.at[o, q, k], d_s.at[o, d, k], d_r.at[o, d, k])
+
+    product(0, 0)
+    from_side(3, 0)
+    product(0, 3)
+    from_side(1, 1)
+    product(0, 1)
+    for k in (0, 3, 1, 2):
+        landed(arrived.at[0, 2, k], fw_s.at[0, k], fw_r.at[0, k])
+    product(0, 2)
+    product(1, 0)
+    product(1, 3)
+    product(1, 1)
+    for k in (0, 3, 1, 2):
+        landed(arrived.at[1, 2, k], fw_s.at[1, k], fw_r.at[1, k])
+    product(1, 2)
+
+    def give_back(o, q, k, block):
+        if q == 0:
+            back[o, k, 0] = block
+            return
+        answers[o, q - 1, k] = block
+        mine = answers.at[o, q - 1, k]
+        if q == 2:
+            way = 1 if k < 2 else 3
+            send(mine, relay_back.at[o, k], bl_s.at[o, k], bl_r.at[o, k], second(o, way))
+        else:
+            d = 0 if q == 1 else 1
+            send(mine, back.at[o, k, SIDE - q], b_s.at[o, d, k], b_r.at[o, d, k], second(o, q))
+
+    def pass_back(o, k):
+        landed(relay_back.at[o, k], bl_s.at[o, k], bl_r.at[o, k])
+        way = 1 if k < 2 else 3
+        send(relay_back.at[o, k], back.at[o, k, 2], bf_s.at[o, k], bf_r.at[o, k], second(o, way))
+
+    for dx in (2, 1, 3, 0):
+        g = acc_g[:, dx].reshape(SIDE * CAP, 512)
+        u = acc_u[:, dx].reshape(SIDE * CAP, 512)
+        hidden = (g / (1.0 + jnp.exp(-g)) * u).astype(bf16)
+        for o in (0, 1):
+            ans = jnp.dot(
+                hidden, wd[:, o * HALF:(o + 1) * HALF], preferred_element_type=f32
+            ).astype(bf16)
+            for dy in (2, 1, 3, 0):
+                block = ans[dy * CAP:(dy + 1) * CAP]
+                if o == 0:
+                    give_back(0, dy, dx, block)
+                else:
+                    give_back(1, dx, dy, block)
+
+    def choose(o, k, part):
+        rows = []
+        for j in range(SIDE):
+            e = expert_at(o, j)
+            w = weight_row(o, k, e)
+            high = w.astype(bf16).astype(f32)
+            value = high if part == 0 else w - high
+            rows.append(jnp.where(lanes == slot_row(o, k, e), value, 0.0).astype(bf16))
+        return jnp.concatenate(rows, 0)
+
+    def combine(o, k):
+        for j, d in ((3, 0), (1, 1)):
+            landed(back.at[o, k, j], b_s.at[o, d, k], b_r.at[o, d, k])
+        landed(back.at[o, k, 2], bf_s.at[o, k], bf_r.at[o, k])
+        rows = back[o, k].reshape(SIDE * CAP, HALF)
+        dims = (((0,), (0,)), ((), ()))
+        total = lax.dot_general(choose(o, k, 0), rows, dims, preferred_element_type=f32)
+        return total + lax.dot_general(choose(o, k, 1), rows, dims, preferred_element_type=f32)
+
+    for k in (2, 1, 3, 0):
+        for o in (0, 1):
+            pass_back(o, k)
+    for k in (2, 1, 3):
+        for o in (0, 1):
+            partial[o, k - 1] = combine(o, k).astype(bf16)
+            mine = partial.at[o, k - 1]
+            if k == 2:
+                send(mine.at[0:64], relay_part.at[o, 0], p_s.at[o, 2], p_r.at[o, 2], first(o, 1))
+                send(mine.at[64:128], relay_part.at[o, 1], p_s.at[o, 3], p_r.at[o, 3], first(o, 3))
+            elif k == 1:
+                send(mine, part_in.at[o, 2], p_s.at[o, 0], p_r.at[o, 0], first(o, 1))
+            else:
+                send(mine, part_in.at[o, 0], p_s.at[o, 1], p_r.at[o, 1], first(o, 3))
+    for o in (0, 1):
+        landed(relay_part.at[o, 0], p_s.at[o, 2], p_r.at[o, 2])
+        send(relay_part.at[o, 0], part_in.at[o, 1, 0:64], p_s.at[o, 4], p_r.at[o, 4], first(o, 1))
+        landed(relay_part.at[o, 1], p_s.at[o, 3], p_r.at[o, 3])
+        send(relay_part.at[o, 1], part_in.at[o, 1, 64:128], p_s.at[o, 5], p_r.at[o, 5], first(o, 3))
+    for o in (0, 1):
+        kept[:, o * HALF:(o + 1) * HALF] = combine(o, 0)
+    for o in (0, 1):
+        landed(part_in.at[o, 2], p_s.at[o, 0], p_r.at[o, 0])
+        landed(part_in.at[o, 0], p_s.at[o, 1], p_r.at[o, 1])
+        landed(part_in.at[o, 1, 0:64], p_s.at[o, 4], p_r.at[o, 4])
+        landed(part_in.at[o, 1, 64:128], p_s.at[o, 5], p_r.at[o, 5])
+        here = slice(o * HALF, (o + 1) * HALF)
+        kept[:, here] = (
+            kept[:, here] + part_in[o, 0].astype(f32) + part_in[o, 1].astype(f32) + part_in[o, 2].astype(f32)
+        )
+    values = RESIDUAL_SCALE * normed[...].astype(f32) + kept[...] + shared[...]
+    out[...] = (normalize(values) * gain[...]).astype(bf16)
+    for copy in sent:
+        copy.wait_send()
+
+
+def experts(normed, table, gain, w_gate, w_up, w_down, s_gate, s_up, s_down):
+    bf16, f32 = jnp.bfloat16, jnp.float32
+    dma = pltpu.SemaphoreType.DMA
+    vmem = pl.BlockSpec(memory_space=pltpu.VMEM)
+    hbm = pl.BlockSpec(memory_space=pl.ANY)
+    block = (CAP, HALF)
+    return pl.pallas_call(
+        expert_kernel,
+        out_shape=jax.ShapeDtypeStruct(normed.shape, bf16),
+        in_specs=[vmem, vmem, vmem, hbm, hbm, hbm, hbm, hbm, hbm],
+        out_specs=vmem,
+        scratch_shapes=[
+            pltpu.VMEM(w_gate.shape, bf16),
+            pltpu.VMEM(w_up.shape, bf16),
+            pltpu.VMEM(w_down.shape, bf16),
+            pltpu.VMEM(s_gate.shape, bf16),
+            pltpu.VMEM(s_up.shape, bf16),
+            pltpu.VMEM(s_down.shape, bf16),
+            pltpu.VMEM((2, 4, 128, HALF), bf16),
+            pltpu.VMEM((2, 4, 32, 1, 128), f32),
+            pltpu.VMEM((2, 3, 4) + block, bf16),
+            pltpu.VMEM((2, 4) + block, bf16),
+            pltpu.VMEM((2, 4, 4) + block, bf16),
+            pltpu.VMEM((4, 4, CAP, 512), f32),
+            pltpu.VMEM((4, 4, CAP, 512), f32),
+            pltpu.VMEM((2, 3, 4) + block, bf16),
+            pltpu.VMEM((2, 4) + block, bf16),
+            pltpu.VMEM((2, 4, 4) + block, bf16),
+            pltpu.VMEM((2, 3, 128, HALF), bf16),
+            pltpu.VMEM((2, 2) + block, bf16),
+            pltpu.VMEM((2, 3, 128, HALF), bf16),
+            pltpu.VMEM((128, 2048), f32),
+            pltpu.VMEM((128, 2048), f32),
+            dma((6,)),
+            dma((2, 4)), dma((2, 4)), dma((2, 3)), dma((2, 3)),
+            dma((2, 2, 4)), dma((2, 2, 4)), dma((2, 4)), dma((2, 4)), dma((2, 4)), dma((2, 4)),
+            dma((2, 2, 4)), dma((2, 2, 4)), dma((2, 4)), dma((2, 4)), dma((2, 4)), dma((2, 4)),
+            dma((2, 6)), dma((2, 6)),
+        ],
+        compiler_params=pltpu.CompilerParams(
+            collective_id=0, has_side_effects=True, vmem_limit_bytes=60 * 1024 * 1024
+        ),
+    )(normed, table, gain, w_gate, w_up, w_down, s_gate, s_up, s_down)
 
 
 def shards(
@@ -98,46 +393,17 @@
     normed = (
         normalize(RESIDUAL_SCALE * residual.astype(jnp.float32) + projected) * mix_gain
     ).astype(jnp.bfloat16)
-    rows = normed.shape[0]
-    width_full = normed.shape[1]
-    chosen = expert_ids.shape[1]
-    experts_all = lax.axis_size("sp") * expert_gate.shape[0]
-    capacity = min(rows, 4 * rows * chosen // experts_all)
-    flat_ids = expert_ids.reshape(-1)
-    onehot = (flat_ids[:, None] == jnp.arange(experts_all, dtype=jnp.int32)[None, :]).astype(
-        jnp.int32
+    names = jnp.arange(16, dtype=jnp.int32)
+    named = expert_ids[None, :, :] == names[:, None, None]
+    hits = jnp.any(named, 2)
+    ranks = jnp.cumsum(hits.astype(jnp.int32), 1) - 1
+    slots = jnp.where(hits, ranks, -1).astype(jnp.float32)
+    weights = jnp.sum(jnp.where(named, route_weights[None], 0.0), 2)
+    table = jnp.concatenate([slots, weights], 0)[:, None, :]
+    return experts(
+        normed, table, final_gain[None, :], expert_gate[0], expert_up[0], expert_down[0],
+        shared_gate, shared_up, shared_down,
     )
-    earlier = jnp.cumsum(onehot, 0) - onehot
-    ranks = jnp.sum(earlier * onehot, 1)
-    slots = flat_ids * capacity + ranks
-    places = jnp.arange(experts_all * capacity, dtype=jnp.int32)[:, None] == slots[None, :]
-    chooser = jnp.any(places.reshape(experts_all * capacity, rows, chosen), 2).astype(jnp.bfloat16)
-    outgoing = jnp.dot(chooser, normed, preferred_element_type=jnp.float32).astype(jnp.bfloat16)
-    outgoing = outgoing.reshape(experts_all, capacity, width_full)
-    arrived = lax.all_to_all(outgoing, "sp", split_axis=0, concat_axis=0, tiled=True)
-    sources, items, width = arrived.shape
-    flat = arrived.reshape(sources * items, width)
-    hidden = (
-        jax.nn.silu(jnp.dot(flat, expert_gate[0], preferred_element_type=jnp.float32))
-        * jnp.dot(flat, expert_up[0], preferred_element_type=jnp.float32)
-    ).astype(jnp.bfloat16)
-    answer = jnp.dot(hidden, expert_down[0], preferred_element_type=jnp.float32).astype(
-        jnp.bfloat16
-    )
-    answered = answer.reshape(sources, items, width)
-    returned = lax.all_to_all(answered, "sp", split_axis=0, concat_axis=0, tiled=True).reshape(
-        experts_all * capacity, width_full
-    )
-    picked = jnp.take(returned, slots, axis=0).astype(jnp.float32).reshape(rows, chosen, width_full)
-    routed = jnp.sum(picked * route_weights[:, :, None], 1)
-    common = (
-        jax.nn.silu(jnp.dot(normed, shared_gate, preferred_element_type=jnp.float32))
-        * jnp.dot(normed, shared_up, preferred_element_type=jnp.float32)
-    ).astype(jnp.bfloat16)
-    shared_out = jnp.dot(common, shared_down, preferred_element_type=jnp.float32)
-    return (
-        normalize(RESIDUAL_SCALE * normed.astype(jnp.float32) + routed + shared_out) * final_gain
-    ).astype(jnp.bfloat16)
 
 
 def solution(mesh):

time: 253 us -> 175 us (0.69)
  Pallas kernels: 0 us -> 79.5 us
  waiting for transfers between devices: 93.8 us -> 30.2 us
  blocking collectives: 62.2 us -> 5.02 us
  matrix products: 25 us -> 4.78 us
  local copies, waits for them, and re-layouts: 13.8 us -> 3.79 us
  starting transfers between devices: 20.1 us -> 15.2 us
    pallas_call x0 -> x1, Pallas kernels: none -> 79.5 us  [experts(): pl.pallas_call(expert_kernel, out_shape=jax.ShapeDtypeStruct(normed.shape...]
    all_to_all x1 -> x0, waiting for transfers between devices: 58.3 us -> none  [shards(): lax.all_to_all(answered, 'sp', split_axis=0, concat_axis=0, tiled=True)]
    all_to_all x1 -> x0, blocking collectives: 56.6 us -> none  [shards(): lax.all_to_all(outgoing, 'sp', split_axis=0, concat_axis=0, tiled=True)]
    dot_general x5 -> x0, matrix products: 20.2 us -> none  [the longest x1 10 us: shards(): jnp.dot(hidden, expert_down[0], preferred_element_type=jnp.float32)]
    gather x2 -> x0, local copies, waits for them, and re-layouts: 8.62 us -> none  [shards(): jnp.take(returned, slots, axis=0).astype(jnp.float32)]
    reduce_sum x2 -> x1, other arithmetic: 6.48 us -> 0.71 us  [shards(): weights = jnp.sum(jnp.where(named, route_weights[None], 0.0), 2)]
    all_to_all x1 -> x0, starting transfers between devices: 4.66 us -> none  [shards(): lax.all_to_all(answered, 'sp', split_axis=0, concat_axis=0, tiled=True)]
    all_gather x1, waiting for transfers between devices: 12.7 us -> 8.4 us  [shards(): full_weight = lax.all_gather(output_weight, TP, axis=0, tiled=True)]
  transfers between devices with their start and end apart: 5 -> 4, of which waited for: 4 -> 2; matrix products, arithmetic and copies ran while one was open for 8% -> 13% of each run, Pallas kernels for 0% -> 0%
where the time goes in v1:
time: 175 us
  Pallas kernels  79.5 us (45%)
  waiting for transfers between devices  30.2 us (17%)
  other arithmetic  22.5 us (13%)
  starting transfers between devices  15.2 us (9%)
  between operations  13.5 us (8%)
  blocking collectives  5.02 us (3%)
  matrix products  4.78 us (3%)
  local copies, waits for them, and re-layouts  3.79 us (2%)
    pallas_call x1, Pallas kernels, experts(): pl.pallas_call(expert_kernel, out_shape=jax.ShapeDtypeStruct(normed.shape...  79.5 us
    all_to_all x1, waiting for transfers between devices, exchange_in_order(): whole = lax.all_to_all(whole, axes[k], k, k, tiled=True)  21 us
    convert_element_type x1, other arithmetic, shards(): convolved = total.astype(jnp.bfloat16)  11.2 us
    all_gather x1, waiting for transfers between devices, shards(): full_weight = lax.all_gather(output_weight, TP, axis=0, tiled=True)  8.4 us
    all_to_all x1, starting transfers between devices, exchange_in_order(): whole = lax.all_to_all(whole, axes[k], k, k, tiled=True)  8.19 us
    ppermute x2, starting transfers between devices, passed_along(): return lax.ppermute(block, axis, route)  7.04 us
    all_to_all x1, blocking collectives, exchange_in_order(): whole = lax.all_to_all(whole, axes[k], k, k, tiled=True)  5.02 us
    dot_general x1, matrix products, shards(): jnp.dot(activated, full_weight, preferred_element_type=jnp.float32)  4.78 us
  transfers between devices with their start and end apart: 4, of which 2 were waited for; matrix products, arithmetic and copies ran while one was open for 13% of the time, Pallas kernels for 0%

profile of v1, /device:TPU:1, one launch (start us, length us, event | category | flops | bytes accessed | tf_op | source)
XLA Modules:
  0.0 174.5 jit_solution(11246925268713173023)
XLA Ops:
  6.5 0.0 copy-start
  6.5 0.0 all-gather.2.cloned.1.call-start
  6.5 0.7 all-gather.2.cloned.1.call-update
  7.3 0.8 slice.280
  8.0 3.9 %collective-permute-start = (s32[30]{0:T(128)S(1)}, s32[30]{0:T(128)S(1)}, u32[]{:S(2)}, u32[]{:S(2)}) collective-permute-start(s32[30]{0:T(128)S(1)} %slice.280), channel_id=1, source_target_pairs={{0,16},{16,32},{32,48},{48,64},{64,80},{80,96},{96,112},{112,128},... | collective-permute-start | bytes 368 | tf_op jit(solution)/shard_map/ppermute | solution.py:20
  11.9 1.5 multiply_convert_fusion.2
  13.4 3.1 %collective-permute-start.1 = (bf16[30,128]{1,0:T(8,128)(2,1)S(1)}, bf16[30,128]{1,0:T(8,128)(2,1)S(1)}, u32[]{:S(2)}, u32[]{:S(2)}) collective-permute-start(bf16[30,128]{1,0:T(8,128)(2,1)S(1)} %slice.375), channel_id=1, source_target_pairs={{0,16},{16,32},{32,48},{48,64},{64,80},{80,96},{96,112},{112,128},... | collective-permute-start | bytes 23048 | tf_op jit(solution)/shard_map/ppermute | solution.py:20
  16.6 0.7 convert_element_type.146
  17.3 0.0 collective-permute-done
  17.3 1.2 fusion.35
  18.5 1.2 fusion.37
  19.7 1.2 fusion.39
  20.8 0.9 fusion.89
  21.8 0.0 collective-permute-done.1
  21.8 11.2 %add_convert_fusion = bf16[2048,128]{1,0:T(8,128)(2,1)S(1)} fusion(bf16[2048,128]{1,0:T(8,128)(2,1)S(1)} %multiply_convert_fusion.2, bf16[30,128]{1,0:T(8,128)(2,1)S(1)} %collective-permute-done.1, f32[128]{0:T(128)S(1)} %get-tuple-element.10, f32[128]{0:T(128)S(1)} %get-tuple-element.11, f32[128]{0:T(128)S(1)} %get-tuple-element.12, ...), kind=kLoop, calls=%fused_computation.37 | loop fusion | flops 55836672 | bytes 1133568 | tf_op jit(solution)/shard_map/convert_element_type | solution.py:386
  33.0 0.3 copy.34
  33.3 5.0 %all_to_all.10 = bf16[8,2,128,128]{2,3,0,1:T(8,128)(2,1)S(1)} all-to-all(bf16[8,2,128,128]{2,3,0,1:T(8,128)(2,1)S(1)} %copy.34), channel_id=1, replica_groups=mesh['sp'=16,'tp_0'=8,'tp_1'=2] {'tp_1'}, dimensions={1} | all-to-all | bytes 1048576 | tf_op jit(solution)/shard_map/all_to_all | solution.py:38
  38.3 0.8 copy.35
  39.1 8.2 %all-to-all-start.1 = ((bf16[8,2,128,128]{2,3,1,0:T(8,128)(2,1)}), bf16[8,2,128,128]{2,3,1,0:T(8,128)(2,1)S(1)}, u32[]{:S(2)}, u32[]{:S(2)}) async-start(bf16[8,2,128,128]{2,3,1,0:T(8,128)(2,1)} %copy.35), calls=%async_computation.1 | async-start | bytes 1048576 | tf_op jit(solution)/shard_map/all_to_all | solution.py:38
  47.3 0.7 fusion.31
  48.0 0.3 reduce_window_sum.11
  48.3 0.7 select_reduce_fusion
  49.0 0.6 pad_maximum_fusion.1
  49.6 21.0 %all-to-all-done.1 = bf16[8,2,128,128]{2,3,1,0:T(8,128)(2,1)S(1)} async-done(((bf16[8,2,128,128]{2,3,1,0:T(8,128)(2,1)}), bf16[8,2,128,128]{2,3,1,0:T(8,128)(2,1)S(1)}, u32[]{:S(2)}, u32[]{:S(2)}) %all-to-all-start.1) | async-done | bytes 524320 | tf_op jit(solution)/shard_map/all_to_all | solution.py:38
  70.7 0.3 convert_reduce_fusion
  71.0 1.1 multiply_convert_fusion.1
  72.0 0.0 copy-start.1
  72.1 8.4 %all-gather.2.cloned.1.call-done = bf16[2048,2048]{1,0:T(8,128)(2,1)} async-done(((bf16[128,2048]{1,0:T(8,128)(2,1)}), bf16[2048,2048]{1,0:T(8,128)(2,1)}) %all-gather.2.cloned.1.call-update) | async-done | bytes 8388624 | tf_op jit(solution)/shard_map/all_gather | solution.py:391
  80.5 0.0 copy-done
  80.5 4.8 %fusion.91 = (f32[128]{0:T(128)S(1)}, f32[128]{0:T(128)S(1)}, f32[128,2048]{1,0:T(8,128)S(1)}) fusion(bf16[128,2048]{0,1:T(8,128)(2,1)S(1)} %multiply_convert_fusion.1, bf16[2048,2048]{1,0:T(8,128)(2,1)} %all-gather.2.cloned.1.call-done, bf16[128,2048]{1,0:T(8,128)(2,1)S(1)} %copy-done), kind=kOutput, calls=%fused_computation.232 | convolution fusion | flops 1075314432 | bytes 10486784 | tf_op jit(solution)/shard_map/dot_general | solution.py:392
  85.3 0.0 copy-done.1
  85.3 1.0 multiply_convert_fusion.normed
  86.3 79.5 %shard_map.163 = bf16[128,2048]{1,0:T(8,128)(2,1)} custom-call(bf16[128,2048]{1,0:T(8,128)(2,1)} %multiply_convert_fusion.normed, f32[32,1,128]{2,1,0:T(1,128)} %bitcast.86, f32[1,2048]{1,0:T(1,128)} %bitcast.87, bf16[2048,512]{1,0:T(8,128)(2,1)} %bitcast.83, bf16[2048,512]{1,0:T(8,128)(2,1)} %bitcast.84, bf16[512,2048]{1,0:T(8,128)(2,1)} %bitcast.85, ...), custom_call_target="tpu_custom_call" | custom-call | tf_op jit(solution)/shard_map/pallas_call | solution.py:307
  165.8 1.9 %copy.37 = bf16[128,2048]{1,0:T(8,128)(2,1)} copy(bf16[128,2048]{1,0:T(8,128)(2,1)} %shard_map.163) | data formatting | bytes 1048576
  (7 shorter events, 0.1 us)
Async XLA Ops:
  6.5 73.9 %copy-start = (bf16[128,2048]{1,0:T(8,128)(2,1)S(1)}, bf16[128,2048]{1,0:T(8,128)(2,1)}, u32[]{:S(2)}) copy-start(bf16[128,2048]{1,0:T(8,128)(2,1)} %param.22) | copy-start | bytes 1572868
  6.5 73.9 %all-gather.2.cloned.1.call-start = ((), (), s32[]{:S(2)}) async-start(), calls=%async_computation.2 | async-start | bytes 8912896 | tf_op jit(solution)/shard_map/all_gather | solution.py:391
  8.0 9.3 %collective-permute-start = (s32[30]{0:T(128)S(1)}, s32[30]{0:T(128)S(1)}, u32[]{:S(2)}, u32[]{:S(2)}) collective-permute-start(s32[30]{0:T(128)S(1)} %slice.280), channel_id=1, source_target_pairs={{0,16},{16,32},{32,48},{48,64},{64,80},{80,96},{96,112},{112,128},... | collective-permute-start | bytes 368 | tf_op jit(solution)/shard_map/ppermute | solution.py:20
  13.4 8.3 %collective-permute-start.1 = (bf16[30,128]{1,0:T(8,128)(2,1)S(1)}, bf16[30,128]{1,0:T(8,128)(2,1)S(1)}, u32[]{:S(2)}, u32[]{:S(2)}) collective-permute-start(bf16[30,128]{1,0:T(8,128)(2,1)S(1)} %slice.375), channel_id=1, source_target_pairs={{0,16},{16,32},{32,48},{48,64},{64,80},{80,96},{96,112},{112,128},... | collective-permute-start | bytes 23048 | tf_op jit(solution)/shard_map/ppermute | solution.py:20
  39.1 31.5 %all-to-all-start.1 = ((bf16[8,2,128,128]{2,3,1,0:T(8,128)(2,1)}), bf16[8,2,128,128]{2,3,1,0:T(8,128)(2,1)S(1)}, u32[]{:S(2)}, u32[]{:S(2)}) async-start(bf16[8,2,128,128]{2,3,1,0:T(8,128)(2,1)} %copy.35), calls=%async_computation.1 | async-start | bytes 1048576 | tf_op jit(solution)/shard_map/all_to_all | solution.py:38
  72.0 13.2 %copy-start.1 = (f32[2048]{0:T(1024)S(1)}, f32[2048]{0:T(1024)}, u32[]{:S(2)}) copy-start(f32[2048]{0:T(1024)} %param.23) | copy-start | bytes 24580
Sparse Core Ops, SparseCore 0:
  9.2 71.2 all-gather.1

commit v2 on v1

--- a/solution.py
+++ b/solution.py
@@ -3,45 +3,20 @@
 from jax import lax
 from jax.experimental import pallas as pl
 from jax.experimental.pallas import tpu as pltpu
-from jax.sharding import Mesh
 from jax.sharding import PartitionSpec as P
-
-TP = ("tp_0", "tp_1")
-SP_TP = ("sp", "tp_0", "tp_1")
-
 
 EPSILON = 1e-05
 RESIDUAL_SCALE = 8.0**0.25
-
-
-def passed_along(block, axis, distance):
-    devices = range(lax.axis_size(axis))
-    route = [(i - distance, i) for i in devices if i - distance in devices]
-    return lax.ppermute(block, axis, route)
-
-
-def cut_along(x, dim, length):
-    before, after = (x.shape[:dim], x.shape[dim + 1 :])
-    return jnp.moveaxis(x.reshape(*before, length, -1, *after), dim, 0)
-
-
-def laid_out(tiles, dim):
-    lengths = list(tiles.shape[1:])
-    lengths[dim] *= tiles.shape[0]
-    return jnp.moveaxis(tiles, 0, dim).reshape(lengths)
-
-
-def exchange_in_order(tiles, axes, turns):
-    inside = tiles.shape[1:]
-    whole = tiles.reshape(*(lax.axis_size(a) for a in axes), *inside)
-    for k in turns:
-        whole = lax.all_to_all(whole, axes[k], k, k, tiled=True)
-    return whole.reshape(-1, *inside)
-
-
-def exchange_by_axis(x, axes, turns, split_dim, concat_dim):
-    tiles = cut_along(x, split_dim, lax.axis_size(axes))
-    return laid_out(exchange_in_order(tiles, axes, turns), concat_dim)
+MESH_ID = pl.DeviceIdType.MESH
+HALF = 1024
+SIDE = 4
+DEPTH = 8
+CAP = 64
+ROWS = 128
+HALO = 32
+TAPS = 31
+PLACE = {0: 0, 1: 1, 7: 2, 2: 3, 6: 4, 3: 5, 5: 6, 4: 7}
+GROUP = ((1, 5), (5, 8))
 
 
 def normalize(values):
@@ -50,23 +25,23 @@
     return (values - mean) * lax.rsqrt(square - mean * mean + EPSILON)
 
 
-MESH_ID = pl.DeviceIdType.MESH
-HALF = 1024
-SIDE = 4
-CAP = 64
-
-
-def expert_kernel(
-    normed, table, gain, w_gate, w_up, w_down, s_gate, s_up, s_down, out,
+def layer_kernel(
+    linear_h, gate_h, taps, channel_gain, w_h, residual_h, mix_gain, docs, ids, ways, gain,
+    w_gate, w_up, w_down, s_gate, s_up, s_down, out,
+    linear, gate, residual, weight, gated, tail, tail_docs, halo, halo_docs, tap32, conv, conv_in, act,
+    sums, sums_in, part, part_in2, normed, table,
     wg, wu, wd, sg, su, sd,
     near, meta, packed, relay, arrived, acc_g, acc_u, answers, relay_back, back, partial, relay_part, part_in,
     kept, shared,
+    l_sem, z_s, z_r, h_s, h_r, a_s, a_r, g_s, g_r, f_s, f_r, e_s, e_r, st_s, st_r, x_s, x_r,
     w_sem, s1_s, s1_r, m_s, m_r, d_s, d_r, rl_s, rl_r, fw_s, fw_r,
     b_s, b_r, bl_s, bl_r, bf_s, bf_r, p_s, p_r,
 ):
     f32, bf16 = jnp.float32, jnp.bfloat16
-    sp, tp = lax.axis_index("sp"), (lax.axis_index("tp_0"), lax.axis_index("tp_1"))
+    sp, tp = lax.axis_index("sp"), lax.axis_index("tp")
     y, x = sp // SIDE, sp % SIDE
+    z, core = tp // 2, tp % 2
+    other = 1 - core
 
     def at(dy, dx):
         return ((y + dy) % SIDE) * SIDE + (x + dx) % SIDE
@@ -77,34 +52,259 @@
     def second(o, k):
         return at(k, 0) if o == 0 else at(0, k)
 
-    def send(src, dst, ss, rs, to):
+    def along(dz):
+        return ((z + dz) % DEPTH) * 2 + core
+
+    def push(src, dst, ss, rs, to_sp, to_tp):
         copy = pltpu.make_async_remote_copy(
             src_ref=src, dst_ref=dst, send_sem=ss, recv_sem=rs,
-            device_id=(to, *tp), device_id_type=MESH_ID,
+            device_id=(to_sp, to_tp), device_id_type=MESH_ID,
         )
         copy.start()
         sent.append(copy)
 
+    def send(src, dst, ss, rs, to):
+        push(src, dst, ss, rs, to, tp)
+
     def landed(dst, ss, rs):
         pltpu.make_async_remote_copy(
             src_ref=dst, dst_ref=dst, send_sem=ss, recv_sem=rs,
-            device_id=(first(0, 1), *tp), device_id_type=MESH_ID,
+            device_id=(first(0, 1), tp), device_id_type=MESH_ID,
         ).wait_recv()
 
     sent = []
+    own_loads = [
+        pltpu.make_async_copy(a, b, l_sem.at[i])
+        for i, (a, b) in enumerate(
+            [(w_h, weight.at[0]), (linear_h, linear), (gate_h, gate), (residual_h, residual)]
+        )
+    ]
+    for load in own_loads:
+        load.start()
     loads = [
         pltpu.make_async_copy(a, b, w_sem.at[i])
         for i, (a, b) in enumerate(
             [(s_gate, sg), (s_up, su), (s_down, sd), (w_gate, wg), (w_up, wu), (w_down, wd)]
         )
     ]
+
+    after, ahead = (sp + 1) % 16, (sp + 15) % 16
+    barrier = pltpu.get_barrier_semaphore()
+
+    def greet(to_sp, to_tp):
+        pl.semaphore_signal(barrier, inc=1, device_id=(to_sp, to_tp), device_id_type=MESH_ID)
+
+    for dz in range(1, DEPTH):
+        greet(sp, along(dz))
+    for to in (at(0, 1), at(0, 3), at(1, 0), at(3, 0), after, ahead):
+        greet(to, tp)
+    greet(sp, z * 2 + other)
+    pl.semaphore_wait(barrier, 14)
+
+    def columns(o, k, width=1):
+        fast, slow = (x, y) if o == 0 else (y, x)
+        return pl.ds(pl.multiple_of((slow * SIDE + (fast + k) % SIDE) * 128, 128), 128)
+
+    def side_columns(o, ks, kf):
+        fast, slow = (x, y) if o == 0 else (y, x)
+        block = ((slow + ks) % SIDE) * SIDE + (fast + kf) % SIDE
+        return pl.ds(pl.multiple_of(block * 128, 128), 128)
+
+    own_loads[0].wait()
+    for dz in (7, 1, 6, 2, 5, 3, 4):
+        there = PLACE[(DEPTH - dz) % DEPTH]
+        o = 0 if there < GROUP[0][1] else 1
+        cols = columns(o, 0)
+        push(weight.at[0, :, cols], weight.at[there, :, cols], z_s.at[there], z_r.at[there], sp, along(dz))
+
+    own_loads[1].wait()
+    own_loads[2].wait()
+
+    def gate_rows(a, b):
+        a, b = a.astype(f32), b.astype(f32)
+        return (a * (1.0 / (1.0 + jnp.exp(-b)))).astype(bf16)
+
+    tail[...] = gate_rows(linear[2048 - HALO:, :], gate[2048 - HALO:, :])
+    doc = docs[...]
+    spot = lax.broadcasted_iota(jnp.int32, (16, 128), 0) * 128 + lax.broadcasted_iota(jnp.int32, (16, 128), 1)
+    local, last = [], []
+    for d in (1, 2, 3):
+        below = jnp.where(doc < d, 1.0, 0.0)
+        local.append(jnp.sum(jnp.sum(below, 1, keepdims=True), 0, keepdims=True))
+        below = jnp.where(spot >= 2048 - (TAPS - 1), below, 0.0)
+        last.append(jnp.sum(jnp.sum(below, 1, keepdims=True), 0, keepdims=True))
+    for i in range(3):
+        tail_docs[i:i + 1, :] = jnp.broadcast_to(last[i], (1, 128))
+    tail_docs[3:8, :] = jnp.zeros((5, 128), f32)
+    push(tail, halo, h_s.at[0], h_r.at[0], after, tp)
+    push(tail_docs, halo_docs, h_s.at[1], h_r.at[1], after, tp)
     for load in loads:
         load.start()
 
-    barrier = pltpu.get_barrier_semaphore()
-    for to in (at(0, 1), at(0, 3), at(1, 0), at(3, 0)):
-        pl.semaphore_signal(barrier, inc=1, device_id=(to, *tp), device_id_type=MESH_ID)
-    pl.semaphore_wait(barrier, 4)
+    def gate_block(i, _):
+        rows = pl.ds(pl.multiple_of(i * 128, 128), 128)
+        there = pl.ds(pl.multiple_of(i * 128 + HALO, 32), 128)
+        gated[there, :] = gate_rows(linear[rows, :], gate[rows, :]).astype(f32)
+        return 0
+
+    lax.fori_loop(0, 16, gate_block, 0)
+    tap32[0:TAPS, :] = taps[...].astype(f32)
+
+    def spread(o, k, rows, i):
+        lo, hi = GROUP[o]
+        mine = weight.at[lo:hi, rows, side_columns(o, 0, k)]
+        send(mine, mine, e_s.at[o, k, i], e_r.at[o, k, i], second(o, 1 if i % 2 == 0 else 3))
+
+    whole, upper, lower = slice(0, 128), slice(0, 64), slice(64, 128)
+
+    def gather_start(o):
+        lo, hi = GROUP[o]
+        mine = weight.at[lo:hi, :, columns(o, 0)]
+        for there in range(lo, hi):
+            landed(weight.at[there, :, columns(o, 0)], z_s.at[there], z_r.at[there])
+        send(mine, mine, g_s.at[o, 0], g_r.at[o, 0], first(o, 1))
+        send(mine, mine, g_s.at[o, 1], g_r.at[o, 1], first(o, 3))
+        spread(o, 0, whole, 0)
+        spread(o, 0, whole, 1)
+
+    def gather_near(o):
+        lo, hi = GROUP[o]
+        landed(weight.at[lo:hi, :, columns(o, 3)], g_s.at[o, 0], g_r.at[o, 0])
+        half = weight.at[lo:hi, upper, columns(o, 3)]
+        send(half, half, g_s.at[o, 2], g_r.at[o, 2], first(o, 1))
+        spread(o, 3, whole, 0)
+        spread(o, 3, whole, 1)
+        landed(weight.at[lo:hi, :, columns(o, 1)], g_s.at[o, 1], g_r.at[o, 1])
+        half = weight.at[lo:hi, lower, columns(o, 1)]
+        send(half, half, g_s.at[o, 3], g_r.at[o, 3], first(o, 3))
+        spread(o, 1, whole, 0)
+        spread(o, 1, whole, 1)
+
+    def gather_far(o):
+        lo, hi = GROUP[o]
+        landed(weight.at[lo:hi, upper, columns(o, 2)], g_s.at[o, 2], g_r.at[o, 2])
+        landed(weight.at[lo:hi, lower, columns(o, 2)], g_s.at[o, 3], g_r.at[o, 3])
+        spread(o, 2, whole, 0)
+        spread(o, 2, whole, 1)
+
+    def gather_pass(o):
+        lo, hi = GROUP[o]
+        for k in (0, 3, 1, 2):
+            landed(weight.at[lo:hi, :, side_columns(o, 3, k)], e_s.at[o, k, 0], e_r.at[o, k, 0])
+            half = weight.at[lo:hi, upper, side_columns(o, 3, k)]
+            send(half, half, e_s.at[o, k, 2], e_r.at[o, k, 2], second(o, 1))
+            landed(weight.at[lo:hi, :, side_columns(o, 1, k)], e_s.at[o, k, 1], e_r.at[o, k, 1])
+            half = weight.at[lo:hi, lower, side_columns(o, 1, k)]
+            send(half, half, e_s.at[o, k, 3], e_r.at[o, k, 3], second(o, 3))
+
+    def gather_end(o):
+        lo, hi = GROUP[o]
+        for k in (0, 3, 1, 2):
+            landed(weight.at[lo:hi, upper, side_columns(o, 2, k)], e_s.at[o, k, 2], e_r.at[o, k, 2])
+            landed(weight.at[lo:hi, lower, side_columns(o, 2, k)], e_s.at[o, k, 3], e_r.at[o, k, 3])
+
+    names = lax.broadcasted_iota(jnp.int32, (16, ROWS), 0)
+    hit_0, hit_1 = names == ids[0:1, :], names == ids[1:2, :]
+    hits = jnp.where(hit_0 | hit_1, 1.0, 0.0)
+    before = lax.broadcasted_iota(jnp.int32, (ROWS, ROWS), 0) < lax.broadcasted_iota(jnp.int32, (ROWS, ROWS), 1)
+    ranks = jnp.dot(hits.astype(bf16), jnp.where(before, 1.0, 0.0).astype(bf16), preferred_element_type=f32)
+    slots = jnp.where(hits > 0.5, ranks, -1.0)
+    values = jnp.where(hit_0, ways[0:1, :], 0.0) + jnp.where(hit_1, ways[1:2, :], 0.0)
+    for e in range(16):
+        table[e] = slots[e:e + 1, :]
+        table[e + 16] = values[e:e + 1, :]
+
+    gather_start(0)
+    landed(halo, h_s.at[0], h_r.at[0])
+    landed(halo_docs, h_s.at[1], h_r.at[1])
+    inside = sp > 0
+    gated[0:HALO, :] = jnp.where(inside, halo[...].astype(f32), 0.0)
+    starts = []
+    for i in range(3):
+        extra = jnp.where(inside, halo_docs[i:i + 1, :], float(TAPS - 1)) - float(TAPS - 1)
+        starts.append(local[i] + extra)
+
+    CHUNK = 64
+
+    def conv_block(dz):
+        base = ((z + dz) % DEPTH) * 256
+
+        def piece(i, _):
+            row = pl.multiple_of(base + i * CHUNK, CHUNK)
+            spot = lax.broadcasted_iota(jnp.int32, (CHUNK, 128), 0).astype(f32) + row.astype(f32)
+            begun = jnp.full((CHUNK, 128), -1000.0, f32)
+            for s in starts:
+                begun = jnp.maximum(begun, jnp.where(s <= spot, s, -1000.0))
+            age = spot - begun
+            total = jnp.zeros((CHUNK, 128), f32)
+            for j in range(TAPS):
+                window = gated[pl.ds(row + (HALO - j), CHUNK), :]
+                total = total + jnp.where(age >= float(j), window * tap32[j:j + 1, :], 0.0)
+            conv[pl.ds(row, CHUNK), :] = total.astype(bf16)
+            return 0
+
+        lax.fori_loop(0, 256 // CHUNK, piece, 0)
+        rows = pl.ds(pl.multiple_of(base, 256), 256)
+        if dz == 0:
+            conv_in[:, 0:128] = conv[rows, :]
+        else:
+            there = PLACE[(DEPTH - dz) % DEPTH]
+            push(
+                conv.at[rows, :], conv_in.at[:, there * 128:(there + 1) * 128],
+                a_s.at[there], a_r.at[there], sp, along(dz),
+            )
+
+    for dz in (4, 3, 5):
+        conv_block(dz)
+    gather_near(0)
+    for dz in (2, 6):
+        conv_block(dz)
+    gather_start(1)
+    for dz in (1, 7):
+        conv_block(dz)
+    gather_far(0)
+    conv_block(0)
+    gather_near(1)
+    gather_far(1)
+    gather_pass(0)
+
+    for there in range(1, DEPTH):
+        landed(conv_in.at[:, there * 128:(there + 1) * 128], a_s.at[there], a_r.at[there])
+    mean_part = jnp.zeros((256, 128), f32)
+    square_part = jnp.zeros((256, 128), f32)
+    for s in range(DEPTH):
+        v = conv_in[:, s * 128:(s + 1) * 128].astype(f32)
+        mean_part = mean_part + v
+        square_part = square_part + v * v
+    sums[0] = mean_part
+    sums[1] = square_part
+    push(sums, sums_in, st_s, st_r, sp, z * 2 + other)
+    gather_pass(1)
+    landed(sums_in, st_s, st_r)
+    mean = jnp.sum(sums[0] + sums_in[0], 1, keepdims=True) * (1.0 / 2048.0)
+    square = jnp.sum(sums[1] + sums_in[1], 1, keepdims=True) * (1.0 / 2048.0)
+    scale = lax.rsqrt(square - mean * mean + EPSILON)
+    for dz, s in PLACE.items():
+        v = conv_in[:, s * 128:(s + 1) * 128].astype(f32)
+        v = (v - mean) * scale * channel_gain[along(dz)]
+        act[:, s * 128:(s + 1) * 128] = (v / (1.0 + jnp.exp(-v))).astype(bf16)
+
+    gather_end(0)
+    for n in range(4):
+        w = weight[0:4, :, n * 512:(n + 1) * 512].reshape(512, 512)
+        part[n] = jnp.dot(act[:, 0:512], w, preferred_element_type=f32).reshape(2, ROWS, 512)
+    gather_end(1)
+    for n in range(4):
+        w = weight[4:8, :, n * 512:(n + 1) * 512].reshape(512, 512)
+        got = jnp.dot(act[:, 512:1024], w, preferred_element_type=f32).reshape(2, ROWS, 512)
+        part[n] = part[n] + got
+        push(part.at[n, other], part_in2.at[n], x_s.at[n], x_r.at[n], sp, z * 2 + other)
+    own_loads[3].wait()
+    for n in range(4):
+        cols = slice(n * 512, (n + 1) * 512)
+        landed(part_in2.at[n], x_s.at[n], x_r.at[n])
+        kept[:, cols] = RESIDUAL_SCALE * residual[:, cols].astype(f32) + part[n, core] + part_in2[n]
+    normed[...] = (normalize(kept[...]) * mix_gain[...]).astype(bf16)
 
     for o in (0, 1):
         mine = normed.at[:, o * HALF:(o + 1) * HALF]
@@ -298,25 +498,55 @@
         copy.wait_send()
 
 
-def experts(normed, table, gain, w_gate, w_up, w_down, s_gate, s_up, s_down):
+def shards(
+    linear_part, gate_part, kernel_taps, channel_gain, output_weight, residual, mix_gain, documents,
+    expert_ids, route_weights, expert_gate, expert_up, expert_down, shared_gate, shared_up, shared_down,
+    final_gain,
+):
     bf16, f32 = jnp.bfloat16, jnp.float32
     dma = pltpu.SemaphoreType.DMA
     vmem = pl.BlockSpec(memory_space=pltpu.VMEM)
     hbm = pl.BlockSpec(memory_space=pl.ANY)
     block = (CAP, HALF)
+    w_gate, w_up, w_down = expert_gate[0], expert_up[0], expert_down[0]
+    args = (
+        (linear_part, hbm), (gate_part, hbm), (kernel_taps, vmem), (channel_gain.reshape(16, 1, 128), vmem),
+        (output_weight, hbm), (residual, hbm), (mix_gain[None, :], vmem), (documents.reshape(16, 128), vmem),
+        (expert_ids.T, vmem), (route_weights.T, vmem), (final_gain[None, :], vmem),
+        (w_gate, hbm), (w_up, hbm), (w_down, hbm), (shared_gate, hbm), (shared_up, hbm), (shared_down, hbm),
+    )
     return pl.pallas_call(
-        expert_kernel,
-        out_shape=jax.ShapeDtypeStruct(normed.shape, bf16),
-        in_specs=[vmem, vmem, vmem, hbm, hbm, hbm, hbm, hbm, hbm],
+        layer_kernel,
+        out_shape=jax.ShapeDtypeStruct(residual.shape, bf16),
+        in_specs=[spec for _, spec in args],
         out_specs=vmem,
         scratch_shapes=[
+            pltpu.VMEM((2048, 128), bf16),
+            pltpu.VMEM((2048, 128), bf16),
+            pltpu.VMEM((ROWS, 2048), bf16),
+            pltpu.VMEM((DEPTH, 128, 2048), bf16),
+            pltpu.VMEM((2048 + HALO, 128), f32),
+            pltpu.VMEM((HALO, 128), bf16),
+            pltpu.VMEM((8, 128), f32),
+            pltpu.VMEM((HALO, 128), bf16),
+            pltpu.VMEM((8, 128), f32),
+            pltpu.VMEM((32, 128), f32),
+            pltpu.VMEM((2048, 128), bf16),
+            pltpu.VMEM((256, HALF), bf16),
+            pltpu.VMEM((256, HALF), bf16),
+            pltpu.VMEM((2, 256, 128), f32),
+            pltpu.VMEM((2, 256, 128), f32),
+            pltpu.VMEM((4, 2, ROWS, 512), f32),
+            pltpu.VMEM((4, ROWS, 512), f32),
+            pltpu.VMEM((ROWS, 2048), bf16),
+            pltpu.VMEM((32, 1, 128), f32),
             pltpu.VMEM(w_gate.shape, bf16),
             pltpu.VMEM(w_up.shape, bf16),
             pltpu.VMEM(w_down.shape, bf16),
-            pltpu.VMEM(s_gate.shape, bf16),
-            pltpu.VMEM(s_up.shape, bf16),
-            pltpu.VMEM(s_down.shape, bf16),
-            pltpu.VMEM((2, 4, 128, HALF), bf16),
+            pltpu.VMEM(shared_gate.shape, bf16),
+            pltpu.VMEM(shared_up.shape, bf16),
+            pltpu.VMEM(shared_down.shape, bf16),
+            pltpu.VMEM((2, 4, ROWS, HALF), bf16),
             pltpu.VMEM((2, 4, 32, 1, 128), f32),
             pltpu.VMEM((2, 3, 4) + block, bf16),
             pltpu.VMEM((2, 4) + block, bf16),
@@ -326,11 +556,14 @@
             pltpu.VMEM((2, 3, 4) + block, bf16),
             pltpu.VMEM((2, 4) + block, bf16),
             pltpu.VMEM((2, 4, 4) + block, bf16),
-            pltpu.VMEM((2, 3, 128, HALF), bf16),
+            pltpu.VMEM((2, 3, ROWS, HALF), bf16),
             pltpu.VMEM((2, 2) + block, bf16),
-            pltpu.VMEM((2, 3, 128, HALF), bf16),
-            pltpu.VMEM((128, 2048), f32),
-            pltpu.VMEM((128, 2048), f32),
+            pltpu.VMEM((2, 3, ROWS, HALF), bf16),
+            pltpu.VMEM((ROWS, 2048), f32),
+            pltpu.VMEM((ROWS, 2048), f32),
+            dma((4,)), dma((8,)), dma((8,)), dma((2,)), dma((2,)), dma((8,)), dma((8,)),
+            dma((2, 4)), dma((2, 4)), dma((1,)), dma((1,)), dma((2, 4, 4)), dma((2, 4, 4)),
+            dma, dma, dma((4,)), dma((4,)),
             dma((6,)),
             dma((2, 4)), dma((2, 4)), dma((2, 3)), dma((2, 3)),
             dma((2, 2, 4)), dma((2, 2, 4)), dma((2, 4)), dma((2, 4)), dma((2, 4)), dma((2, 4)),
@@ -338,95 +571,15 @@
             dma((2, 6)), dma((2, 6)),
         ],
         compiler_params=pltpu.CompilerParams(
-            collective_id=0, has_side_effects=True, vmem_limit_bytes=60 * 1024 * 1024
+            collective_id=0, has_side_effects=True, vmem_limit_bytes=63 * 1024 * 1024
         ),
-    )(normed, table, gain, w_gate, w_up, w_down, s_gate, s_up, s_down)
-
-
-def shards(
-    linear_part,
-    gate_part,
-    kernel_taps,
-    channel_gain,
-    output_weight,
-    residual,
-    mix_gain,
-    documents,
-    expert_ids,
-    route_weights,
-    expert_gate,
-    expert_up,
-    expert_down,
-    shared_gate,
-    shared_up,
-    shared_down,
-    final_gain,
-):
-    reach = kernel_taps.shape[0] - 1
-    length = linear_part.shape[0]
-    gated = (
-        linear_part.astype(jnp.float32) * jax.nn.sigmoid(gate_part.astype(jnp.float32))
-    ).astype(jnp.bfloat16)
-    before, before_docs = passed_along(
-        (gated[length - reach :], documents[length - reach :]), "sp", 1
+    )(*[a for a, _ in args])
+
+
+def solution(mesh):
+    both = P(("sp", "tp"), None)
+    placed = (
+        P("sp", "tp"), P("sp", "tp"), P(None, "tp"), P(), P("tp", None), both, P(), P("sp"), both, both,
+        P("sp", None, None), P("sp", None, None), P("sp", None, None), P(), P(), P(), P(),
     )
-    extended = jnp.concatenate([before, gated], 0)
-    extended_docs = jnp.concatenate([before_docs, documents], 0)
-    taps = kernel_taps.astype(jnp.float32)
-    total = jnp.zeros(gated.shape, jnp.float32)
-    for offset in range(reach + 1):
-        window = lax.slice_in_dim(extended, reach - offset, reach - offset + length, axis=0).astype(
-            jnp.float32
-        )
-        same = (
-            lax.slice_in_dim(extended_docs, reach - offset, reach - offset + length, axis=0)
-            == documents
-        )
-        total = total + jnp.where(same[:, None], window * taps[offset], 0.0)
-    convolved = total.astype(jnp.bfloat16)
-    position_rows = exchange_by_axis(convolved, TP, (1, 0), 0, 1)
-    activated = jax.nn.silu(normalize(position_rows.astype(jnp.float32)) * channel_gain).astype(
-        jnp.bfloat16
-    )
-    full_weight = lax.all_gather(output_weight, TP, axis=0, tiled=True)
-    projected = jnp.dot(activated, full_weight, preferred_element_type=jnp.float32)
-    normed = (
-        normalize(RESIDUAL_SCALE * residual.astype(jnp.float32) + projected) * mix_gain
-    ).astype(jnp.bfloat16)
-    names = jnp.arange(16, dtype=jnp.int32)
-    named = expert_ids[None, :, :] == names[:, None, None]
-    hits = jnp.any(named, 2)
-    ranks = jnp.cumsum(hits.astype(jnp.int32), 1) - 1
-    slots = jnp.where(hits, ranks, -1).astype(jnp.float32)
-    weights = jnp.sum(jnp.where(named, route_weights[None], 0.0), 2)
-    table = jnp.concatenate([slots, weights], 0)[:, None, :]
-    return experts(
-        normed, table, final_gain[None, :], expert_gate[0], expert_up[0], expert_down[0],
-        shared_gate, shared_up, shared_down,
-    )
-
-
-def solution(mesh):
-    finer = Mesh(mesh.devices.reshape(mesh.shape["sp"], 8, 2), ("sp", "tp_0", "tp_1"))
-    placed = (
-        P("sp", TP),
-        P("sp", TP),
-        P(None, TP),
-        P(),
-        P(TP, None),
-        P(SP_TP, None),
-        P(),
-        P("sp"),
-        P(SP_TP, None),
-        P(SP_TP, None),
-        P("sp", None, None),
-        P("sp", None, None),
-        P("sp", None, None),
-        P(),
-        P(),
-        P(),
-        P(),
-    )
-    return jax.shard_map(
-        shards, mesh=finer, in_specs=placed, out_specs=P(SP_TP, None), check_vma=False
-    )
+    return jax.shard_map(shards, mesh=mesh, in_specs=placed, out_specs=both, check_vma=False)

time: 175 us -> 126 us (0.72)
  Pallas kernels: 79.5 us -> 124 us
  waiting for transfers between devices: 30.2 us -> 0 us
  other arithmetic: 22.5 us -> 0 us
  starting transfers between devices: 15.2 us -> 0 us
  between operations: 13.5 us -> 0.01 us
  blocking collectives: 5.02 us -> 0 us
  matrix products: 4.78 us -> 0 us
  local copies, waits for them, and re-layouts: 3.79 us -> 1.88 us
    pallas_call x1, Pallas kernels: 79.5 us -> 124 us  [shards(): pl.pallas_call(layer_kernel, out_shape=jax.ShapeDtypeStruct(residual.shap...]
    all_to_all x1 -> x0, waiting for transfers between devices: 21 us -> none  [exchange_in_order(): whole = lax.all_to_all(whole, axes[k], k, k, tiled=True)]
    convert_element_type x7 -> x0, other arithmetic: 15.5 us -> none  [the longest x1 11.2 us: shards(): convolved = total.astype(jnp.bfloat16)]
    all_gather x1 -> x0, waiting for transfers between devices: 8.4 us -> none  [shards(): full_weight = lax.all_gather(output_weight, TP, axis=0, tiled=True)]
    all_to_all x1 -> x0, starting transfers between devices: 8.19 us -> none  [exchange_in_order(): whole = lax.all_to_all(whole, axes[k], k, k, tiled=True)]
    ppermute x2 -> x0, starting transfers between devices: 7.04 us -> none  [passed_along(): return lax.ppermute(block, axis, route)]
    all_to_all x1 -> x0, blocking collectives: 5.02 us -> none  [exchange_in_order(): whole = lax.all_to_all(whole, axes[k], k, k, tiled=True)]
    dot_general x1 -> x0, matrix products: 4.78 us -> none  [shards(): jnp.dot(activated, full_weight, preferred_element_type=jnp.float32)]
  transfers between devices with their start and end apart: 4 -> 0, of which waited for: 2 -> 0; matrix products, arithmetic and copies ran while one was open for 13% -> 0% of each run, Pallas kernels for 0% -> 0%
where the time goes in v2:
time: 126 us
  Pallas kernels  124 us (98%)
  local copies, waits for them, and re-layouts  1.88 us (1%)
    pallas_call x1, Pallas kernels, shards(): pl.pallas_call(layer_kernel, out_shape=jax.ShapeDtypeStruct(residual.shap...  124 us

profile of v2, /device:TPU:1, one launch (start us, length us, event | category | flops | bytes accessed | tf_op | source)
XLA Modules:
  0.0 126.0 jit_solution(965827004116953377)
XLA Ops:
  0.0 124.1 %shard_map.163 = bf16[128,2048]{1,0:T(8,128)(2,1)} custom-call(bf16[2048,128]{1,0:T(8,128)(2,1)} %linear_h.1, bf16[2048,128]{1,0:T(8,128)(2,1)} %gate_h.1, bf16[31,128]{1,0:T(8,128)(2,1)} %taps.1, f32[16,1,128]{2,1,0:T(1,128)} %bitcast.12, bf16[128,2048]{1,0:T(8,128)(2,1)} %w_h.1, bf16[128,2048]{1,0:T(8,128)(2,1)} %residual_h.1, f32[1,2048]{1,0:T(1,128)} %bitcast.13, ...), custom_call_target="tpu_custom_call" | custom-call | tf_op jit(solution)/shard_map/pallas_call | solution.py:518
  124.1 1.9 %copy.19 = bf16[128,2048]{1,0:T(8,128)(2,1)} copy(bf16[128,2048]{1,0:T(8,128)(2,1)} %shard_map.163) | data formatting | bytes 1048576

commit v3 on v2

--- a/solution.py
+++ b/solution.py
@@ -31,7 +31,7 @@
     linear, gate, residual, weight, gated, tail, tail_docs, halo, halo_docs, tap32, conv, conv_in, act,
     sums, sums_in, part, part_in2, normed, table,
     wg, wu, wd, sg, su, sd,
-    near, meta, packed, relay, arrived, acc_g, acc_u, answers, relay_back, back, partial, relay_part, part_in,
+    near, meta, packed, relay, arrived, acc_g, acc_u, hidden, answers, relay_back, back, partial, relay_part, part_in,
     kept, shared,
     l_sem, z_s, z_r, h_s, h_r, a_s, a_r, g_s, g_r, f_s, f_r, e_s, e_r, st_s, st_r, x_s, x_r,
     w_sem, s1_s, s1_r, m_s, m_r, d_s, d_r, rl_s, rl_r, fw_s, fw_r,
@@ -368,47 +368,40 @@
         landed(near.at[o, 2, 64:128], s1_s.at[o, 3], s1_r.at[o, 3])
         pack(o, 2)
 
+    acc_g[...] = jnp.zeros_like(acc_g)
+    acc_u[...] = jnp.zeros_like(acc_u)
     for load in loads[:3]:
         load.wait()
     act = jnp.dot(normed[...], sg[...], preferred_element_type=f32)
     lin = jnp.dot(normed[...], su[...], preferred_element_type=f32)
     common = (act / (1.0 + jnp.exp(-act)) * lin).astype(bf16)
     shared[...] = jnp.dot(common, sd[...], preferred_element_type=f32)
-    for k in (3, 1, 2):
+    for k in (3, 1):
         for o in (0, 1):
             pass_on(o, k)
     for load in loads[3:]:
         load.wait()
 
-    def product(o, q):
-        rows = arrived[o, q].reshape(SIDE * CAP, HALF)
+    def product(o, k):
+        landed(arrived.at[o, 3, k], d_s.at[o, 0, k], d_r.at[o, 0, k])
+        landed(arrived.at[o, 1, k], d_s.at[o, 1, k], d_r.at[o, 1, k])
+        landed(arrived.at[o, 2, k], fw_s.at[o, k], fw_r.at[o, k])
+        rows = arrived[o, :, k].reshape(SIDE * CAP, HALF)
         for acc, w in ((acc_g, wg), (acc_u, wu)):
             got = jnp.dot(rows, w[o * HALF:(o + 1) * HALF, :], preferred_element_type=f32)
             got = got.reshape(SIDE, CAP, 512)
             if o == 0:
-                acc[q] = got
+                acc[:, k] = acc[:, k] + got
             else:
-                acc[:, q] = acc[:, q] + got
-
-    def from_side(q, d):
-        for k in range(SIDE):
-            for o in (0, 1):
-                landed(arrived.at[o, q, k], d_s.at[o, d, k], d_r.at[o, d, k])
-
-    product(0, 0)
-    from_side(3, 0)
-    product(0, 3)
-    from_side(1, 1)
-    product(0, 1)
-    for k in (0, 3, 1, 2):
-        landed(arrived.at[0, 2, k], fw_s.at[0, k], fw_r.at[0, k])
-    product(0, 2)
-    product(1, 0)
-    product(1, 3)
-    product(1, 1)
-    for k in (0, 3, 1, 2):
-        landed(arrived.at[1, 2, k], fw_s.at[1, k], fw_r.at[1, k])
-    product(1, 2)
+                acc[k] = acc[k] + got
+
+    for o in (0, 1):
+        product(o, 0)
+    for o in (0, 1):
+        pass_on(o, 2)
+    for k in (3, 1, 2):
+        for o in (0, 1):
+            product(o, k)
 
     def give_back(o, q, k, block):
         if q == 0:
@@ -428,20 +421,22 @@
         way = 1 if k < 2 else 3
         send(relay_back.at[o, k], back.at[o, k, 2], bf_s.at[o, k], bf_r.at[o, k], second(o, way))
 
-    for dx in (2, 1, 3, 0):
-        g = acc_g[:, dx].reshape(SIDE * CAP, 512)
-        u = acc_u[:, dx].reshape(SIDE * CAP, 512)
-        hidden = (g / (1.0 + jnp.exp(-g)) * u).astype(bf16)
+    ready = set()
+
+    def hide(dy, dx):
+        if (dy, dx) not in ready:
+            ready.add((dy, dx))
+            g = acc_g[dy, dx]
+            hidden[dy, dx] = (g / (1.0 + jnp.exp(-g)) * acc_u[dy, dx]).astype(bf16)
+
+    for k in (2, 1, 3, 0):
         for o in (0, 1):
-            ans = jnp.dot(
-                hidden, wd[:, o * HALF:(o + 1) * HALF], preferred_element_type=f32
-            ).astype(bf16)
-            for dy in (2, 1, 3, 0):
-                block = ans[dy * CAP:(dy + 1) * CAP]
-                if o == 0:
-                    give_back(0, dy, dx, block)
-                else:
-                    give_back(1, dx, dy, block)
+            for q in range(SIDE):
+                hide(*((q, k) if o == 0 else (k, q)))
+            rows = (hidden[:, k] if o == 0 else hidden[k]).reshape(SIDE * CAP, 512)
+            ans = jnp.dot(rows, wd[:, o * HALF:(o + 1) * HALF], preferred_element_type=f32).astype(bf16)
+            for q in (2, 1, 3, 0):
+                give_back(o, q, k, ans[q * CAP:(q + 1) * CAP])
 
     def choose(o, k, part):
         rows = []
@@ -462,38 +457,38 @@
         total = lax.dot_general(choose(o, k, 0), rows, dims, preferred_element_type=f32)
         return total + lax.dot_general(choose(o, k, 1), rows, dims, preferred_element_type=f32)
 
-    for k in (2, 1, 3, 0):
+    def pass_sum(o, k):
+        total = combine(o, k)
+        mine = partial.at[o, k - 1]
+        if k == 2:
+            partial[o, k - 1] = total.astype(bf16)
+            send(mine.at[0:64], relay_part.at[o, 0], p_s.at[o, 2], p_r.at[o, 2], first(o, 1))
+            send(mine.at[64:128], relay_part.at[o, 1], p_s.at[o, 3], p_r.at[o, 3], first(o, 3))
+        elif k == 1:
+            landed(relay_part.at[o, 0], p_s.at[o, 2], p_r.at[o, 2])
+            partial[o, k - 1, 0:64] = (total[0:64] + relay_part[o, 0].astype(f32)).astype(bf16)
+            partial[o, k - 1, 64:128] = total[64:128].astype(bf16)
+            send(mine, part_in.at[o, 0], p_s.at[o, 0], p_r.at[o, 0], first(o, 1))
+        else:
+            landed(relay_part.at[o, 1], p_s.at[o, 3], p_r.at[o, 3])
+            partial[o, k - 1, 0:64] = total[0:64].astype(bf16)
+            partial[o, k - 1, 64:128] = (total[64:128] + relay_part[o, 1].astype(f32)).astype(bf16)
+            send(mine, part_in.at[o, 1], p_s.at[o, 1], p_r.at[o, 1], first(o, 3))
+
+    for step, k in (
+        (pass_back, 2), (pass_back, 1), (pass_sum, 2), (pass_back, 3), (pass_sum, 1), (pass_back, 0), (pass_sum, 3)
+    ):
         for o in (0, 1):
-            pass_back(o, k)
-    for k in (2, 1, 3):
-        for o in (0, 1):
-            partial[o, k - 1] = combine(o, k).astype(bf16)
-            mine = partial.at[o, k - 1]
-            if k == 2:
-                send(mine.at[0:64], relay_part.at[o, 0], p_s.at[o, 2], p_r.at[o, 2], first(o, 1))
-                send(mine.at[64:128], relay_part.at[o, 1], p_s.at[o, 3], p_r.at[o, 3], first(o, 3))
-            elif k == 1:
-                send(mine, part_in.at[o, 2], p_s.at[o, 0], p_r.at[o, 0], first(o, 1))
-            else:
-                send(mine, part_in.at[o, 0], p_s.at[o, 1], p_r.at[o, 1], first(o, 3))
-    for o in (0, 1):
-        landed(relay_part.at[o, 0], p_s.at[o, 2], p_r.at[o, 2])
-        send(relay_part.at[o, 0], part_in.at[o, 1, 0:64], p_s.at[o, 4], p_r.at[o, 4], first(o, 1))
-        landed(relay_part.at[o, 1], p_s.at[o, 3], p_r.at[o, 3])
-        send(relay_part.at[o, 1], part_in.at[o, 1, 64:128], p_s.at[o, 5], p_r.at[o, 5], first(o, 3))
+            step(o, k)
     for o in (0, 1):
         kept[:, o * HALF:(o + 1) * HALF] = combine(o, 0)
     for o in (0, 1):
-        landed(part_in.at[o, 2], p_s.at[o, 0], p_r.at[o, 0])
-        landed(part_in.at[o, 0], p_s.at[o, 1], p_r.at[o, 1])
-        landed(part_in.at[o, 1, 0:64], p_s.at[o, 4], p_r.at[o, 4])
-        landed(part_in.at[o, 1, 64:128], p_s.at[o, 5], p_r.at[o, 5])
+        landed(part_in.at[o, 0], p_s.at[o, 0], p_r.at[o, 0])
+        landed(part_in.at[o, 1], p_s.at[o, 1], p_r.at[o, 1])
         here = slice(o * HALF, (o + 1) * HALF)
-        kept[:, here] = (
-            kept[:, here] + part_in[o, 0].astype(f32) + part_in[o, 1].astype(f32) + part_in[o, 2].astype(f32)
-        )
+        kept[:, here] = kept[:, here] + part_in[o, 0].astype(f32) + part_in[o, 1].astype(f32)
     values = RESIDUAL_SCALE * normed[...].astype(f32) + kept[...] + shared[...]
-    out[...] = (normalize(values) * gain[...]).astype(bf16)
+    out[...] = normalize(values) * gain[...]
     for copy in sent:
         copy.wait_send()
 
@@ -517,7 +512,7 @@
     )
     return pl.pallas_call(
         layer_kernel,
-        out_shape=jax.ShapeDtypeStruct(residual.shape, bf16),
+        out_shape=jax.ShapeDtypeStruct(residual.shape, f32),
         in_specs=[spec for _, spec in args],
         out_specs=vmem,
         scratch_shapes=[
@@ -553,12 +548,13 @@
             pltpu.VMEM((2, 4, 4) + block, bf16),
             pltpu.VMEM((4, 4, CAP, 512), f32),
             pltpu.VMEM((4, 4, CAP, 512), f32),
+            pltpu.VMEM((4, 4, CAP, 512), bf16),
             pltpu.VMEM((2, 3, 4) + block, bf16),
             pltpu.VMEM((2, 4) + block, bf16),
             pltpu.VMEM((2, 4, 4) + block, bf16),
             pltpu.VMEM((2, 3, ROWS, HALF), bf16),
             pltpu.VMEM((2, 2) + block, bf16),
-            pltpu.VMEM((2, 3, ROWS, HALF), bf16),
+            pltpu.VMEM((2, 2, ROWS, HALF), bf16),
             pltpu.VMEM((ROWS, 2048), f32),
             pltpu.VMEM((ROWS, 2048), f32),
             dma((4,)), dma((8,)), dma((8,)), dma((2,)), dma((2,)), dma((8,)), dma((8,)),
@@ -568,12 +564,12 @@
             dma((2, 4)), dma((2, 4)), dma((2, 3)), dma((2, 3)),
             dma((2, 2, 4)), dma((2, 2, 4)), dma((2, 4)), dma((2, 4)), dma((2, 4)), dma((2, 4)),
             dma((2, 2, 4)), dma((2, 2, 4)), dma((2, 4)), dma((2, 4)), dma((2, 4)), dma((2, 4)),
-            dma((2, 6)), dma((2, 6)),
+            dma((2, 4)), dma((2, 4)),
         ],
         compiler_params=pltpu.CompilerParams(
             collective_id=0, has_side_effects=True, vmem_limit_bytes=63 * 1024 * 1024
         ),
-    )(*[a for a, _ in args])
+    )(*[a for a, _ in args]).astype(bf16)
 
 
 def solution(mesh):

time: 126 us -> 128 us (1.016)
  other arithmetic: 0 us -> 2.09 us
  local copies, waits for them, and re-layouts: 1.88 us -> 0 us
    convert_element_type x0 -> x1, other arithmetic: none -> 2.09 us  [shards(): return pl.pallas_call(layer_kernel, out_shape=jax.ShapeDtypeStruct(residu...]
    unnamed x1 -> x0, local copies, waits for them, and re-layouts: 1.88 us -> none
    pallas_call x1, Pallas kernels: 124 us -> 125 us  [shards(): pl.pallas_call(layer_kernel, out_shape=jax.ShapeDtypeStruct(residual.shap...]
where the time goes in v3:
time: 128 us
  Pallas kernels  125 us (98%)
  other arithmetic  2.09 us (2%)
    pallas_call x1, Pallas kernels, shards(): pl.pallas_call(layer_kernel, out_shape=jax.ShapeDtypeStruct(residual.shap...  125 us

profile of v3, /device:TPU:1, one launch (start us, length us, event | category | flops | bytes accessed | tf_op | source)
XLA Modules:
  0.0 127.5 jit_solution(10589076860835830824)
XLA Ops:
  0.0 125.4 %shard_map.163 = f32[128,2048]{1,0:T(8,128)} custom-call(bf16[2048,128]{1,0:T(8,128)(2,1)} %linear_h.1, bf16[2048,128]{1,0:T(8,128)(2,1)} %gate_h.1, bf16[31,128]{1,0:T(8,128)(2,1)} %taps.1, f32[16,1,128]{2,1,0:T(1,128)} %bitcast.12, bf16[128,2048]{1,0:T(8,128)(2,1)} %w_h.1, bf16[128,2048]{1,0:T(8,128)(2,1)} %residual_h.1, f32[1,2048]{1,0:T(1,128)} %bitcast.13, ...), custom_call_target="tpu_custom_call" | custom-call | tf_op jit(solution)/shard_map/pallas_call | solution.py:513
  125.5 2.1 %convert_element_type.3 = bf16[128,2048]{1,0:T(8,128)(2,1)} convert(f32[128,2048]{1,0:T(8,128)} %shard_map.163) | non-fusion elementwise | flops 262144 | bytes 1572864 | tf_op jit(solution)/shard_map/convert_element_type | solution.py:572

commit v4 on v3

--- a/solution.py
+++ b/solution.py
@@ -73,6 +73,11 @@
         ).wait_recv()
 
     sent = []
+
+    def drain(keep=0):
+        while len(sent) > keep:
+            sent.pop(0).wait_send()
+
     own_loads = [
         pltpu.make_async_copy(a, b, l_sem.at[i])
         for i, (a, b) in enumerate(
@@ -306,6 +311,7 @@
         kept[:, cols] = RESIDUAL_SCALE * residual[:, cols].astype(f32) + part[n, core] + part_in2[n]
     normed[...] = (normalize(kept[...]) * mix_gain[...]).astype(bf16)
 
+    before_rows = len(sent)
     for o in (0, 1):
         mine = normed.at[:, o * HALF:(o + 1) * HALF]
         send(table, meta.at[o, 3], m_s.at[o, 0], m_r.at[o, 0], first(o, 1))
@@ -348,6 +354,7 @@
 
     for o in (0, 1):
         pack(o, 0)
+    drain(len(sent) - before_rows)
     for o in (0, 1):
         landed(meta.at[o, 3], m_s.at[o, 0], m_r.at[o, 0])
         send(meta.at[o, 3], meta.at[o, 2], m_s.at[o, 2], m_r.at[o, 2], first(o, 1))
@@ -403,18 +410,19 @@
         for o in (0, 1):
             product(o, k)
 
-    def give_back(o, q, k, block):
-        if q == 0:
-            back[o, k, 0] = block
-            return
-        answers[o, q - 1, k] = block
-        mine = answers.at[o, q - 1, k]
-        if q == 2:
+    before_answers = len(sent)
+    def relayed(k):
+        for o in (0, 1):
             way = 1 if k < 2 else 3
-            send(mine, relay_back.at[o, k], bl_s.at[o, k], bl_r.at[o, k], second(o, way))
-        else:
-            d = 0 if q == 1 else 1
-            send(mine, back.at[o, k, SIDE - q], b_s.at[o, d, k], b_r.at[o, d, k], second(o, q))
+            send(answers.at[o, 1, k], relay_back.at[o, k], bl_s.at[o, k], bl_r.at[o, k], second(o, way))
+
+    def direct(k):
+        for o in (0, 1):
+            for q, d in ((1, 0), (3, 1)):
+                send(
+                    answers.at[o, q - 1, k], back.at[o, k, SIDE - q], b_s.at[o, d, k], b_r.at[o, d, k],
+                    second(o, q),
+                )
 
     def pass_back(o, k):
         landed(relay_back.at[o, k], bl_s.at[o, k], bl_r.at[o, k])
@@ -429,14 +437,24 @@
             g = acc_g[dy, dx]
             hidden[dy, dx] = (g / (1.0 + jnp.exp(-g)) * acc_u[dy, dx]).astype(bf16)
 
-    for k in (2, 1, 3, 0):
+    def answer(k):
         for o in (0, 1):
             for q in range(SIDE):
                 hide(*((q, k) if o == 0 else (k, q)))
             rows = (hidden[:, k] if o == 0 else hidden[k]).reshape(SIDE * CAP, 512)
             ans = jnp.dot(rows, wd[:, o * HALF:(o + 1) * HALF], preferred_element_type=f32).astype(bf16)
-            for q in (2, 1, 3, 0):
-                give_back(o, q, k, ans[q * CAP:(q + 1) * CAP])
+            back[o, k, 0] = ans[0:CAP]
+            for q in (1, 2, 3):
+                answers[o, q - 1, k] = ans[q * CAP:(q + 1) * CAP]
+
+    answer(2)
+    relayed(2)
+    direct(2)
+    answer(1)
+    relayed(1)
+    answer(3)
+    relayed(3)
+    answer(0)
 
     def choose(o, k, part):
         rows = []
@@ -475,22 +493,33 @@
             partial[o, k - 1, 64:128] = (total[64:128] + relay_part[o, 1].astype(f32)).astype(bf16)
             send(mine, part_in.at[o, 1], p_s.at[o, 1], p_r.at[o, 1], first(o, 3))
 
-    for step, k in (
-        (pass_back, 2), (pass_back, 1), (pass_sum, 2), (pass_back, 3), (pass_sum, 1), (pass_back, 0), (pass_sum, 3)
-    ):
+    def both(step, k):
         for o in (0, 1):
             step(o, k)
+
+    both(pass_back, 2)
+    direct(1)
+    both(pass_back, 1)
+    direct(3)
+    both(pass_back, 3)
+    relayed(0)
+    drain(len(sent) - before_answers)
+    both(pass_sum, 2)
+    direct(0)
+    both(pass_back, 0)
+    both(pass_sum, 1)
+    both(pass_sum, 3)
     for o in (0, 1):
         kept[:, o * HALF:(o + 1) * HALF] = combine(o, 0)
+    drain(4)
     for o in (0, 1):
         landed(part_in.at[o, 0], p_s.at[o, 0], p_r.at[o, 0])
         landed(part_in.at[o, 1], p_s.at[o, 1], p_r.at[o, 1])
         here = slice(o * HALF, (o + 1) * HALF)
         kept[:, here] = kept[:, here] + part_in[o, 0].astype(f32) + part_in[o, 1].astype(f32)
     values = RESIDUAL_SCALE * normed[...].astype(f32) + kept[...] + shared[...]
-    out[...] = normalize(values) * gain[...]
-    for copy in sent:
-        copy.wait_send()
+    out[...] = (normalize(values) * gain[...]).astype(bf16)
+    drain()
 
 
 def shards(
@@ -501,7 +530,7 @@
     bf16, f32 = jnp.bfloat16, jnp.float32
     dma = pltpu.SemaphoreType.DMA
     vmem = pl.BlockSpec(memory_space=pltpu.VMEM)
-    hbm = pl.BlockSpec(memory_space=pl.ANY)
+    hbm = pl.BlockSpec(memory_space=pltpu.MemorySpace.HBM)
     block = (CAP, HALF)
     w_gate, w_up, w_down = expert_gate[0], expert_up[0], expert_down[0]
     args = (
@@ -512,7 +541,7 @@
     )
     return pl.pallas_call(
         layer_kernel,
-        out_shape=jax.ShapeDtypeStruct(residual.shape, f32),
+        out_shape=jax.ShapeDtypeStruct(residual.shape, bf16),
         in_specs=[spec for _, spec in args],
         out_specs=vmem,
         scratch_shapes=[
@@ -567,9 +596,9 @@
             dma((2, 4)), dma((2, 4)),
         ],
         compiler_params=pltpu.CompilerParams(
-            collective_id=0, has_side_effects=True, vmem_limit_bytes=63 * 1024 * 1024
+            collective_id=0, has_side_effects=True, vmem_limit_bytes=54 * 1024 * 1024
         ),
-    )(*[a for a, _ in args]).astype(bf16)
+    )(*[a for a, _ in args])
 
 
 def solution(mesh):

time: 128 us -> 123 us (0.961)
  Pallas kernels: 125 us -> 120 us
  other arithmetic: 2.09 us -> 0 us
  local copies, waits for them, and re-layouts: 0 us -> 1.88 us
    pallas_call x1, Pallas kernels: 125 us -> 120 us  [shards(): pl.pallas_call(layer_kernel, out_shape=jax.ShapeDtypeStruct(residual.shap...]
    convert_element_type x1 -> x0, other arithmetic: 2.09 us -> none  [shards(): return pl.pallas_call(layer_kernel, out_shape=jax.ShapeDtypeStruct(residu...]
    unnamed x0 -> x1, local copies, waits for them, and re-layouts: none -> 1.88 us
where the time goes in v4:
time: 123 us; the launch traced here: 122 us
  Pallas kernels  120 us (98%)
  local copies, waits for them, and re-layouts  1.88 us (2%)
    pallas_call x1, Pallas kernels, shards(): pl.pallas_call(layer_kernel, out_shape=jax.ShapeDtypeStruct(residual.shap...  120 us

profile of v4, /device:TPU:1, one launch (start us, length us, event | category | flops | bytes accessed | tf_op | source)
XLA Modules:
  0.0 122.4 jit_solution(4763357518189804740)
XLA Ops:
  0.0 120.5 %shard_map.163 = bf16[128,2048]{1,0:T(8,128)(2,1)} custom-call(bf16[2048,128]{1,0:T(8,128)(2,1)} %linear_h.1, bf16[2048,128]{1,0:T(8,128)(2,1)} %gate_h.1, bf16[31,128]{1,0:T(8,128)(2,1)} %taps.1, f32[16,1,128]{2,1,0:T(1,128)} %bitcast.12, bf16[128,2048]{1,0:T(8,128)(2,1)} %w_h.1, bf16[128,2048]{1,0:T(8,128)(2,1)} %residual_h.1, f32[1,2048]{1,0:T(1,128)} %bitcast.13, ...), custom_call_target="tpu_custom_call" | custom-call | tf_op jit(solution)/shard_map/pallas_call | solution.py:542
  120.5 1.9 %copy.19 = bf16[128,2048]{1,0:T(8,128)(2,1)} copy(bf16[128,2048]{1,0:T(8,128)(2,1)} %shard_map.163) | data formatting | bytes 1048576

commit v5 on v4

v5 whole, which is shorter than its diff:
```python
import jax
import jax.numpy as jnp
from jax import lax
from jax.experimental import pallas as pl
from jax.experimental.pallas import tpu as pltpu
from jax.sharding import PartitionSpec as P

EPSILON = 1e-05
RESIDUAL_SCALE = 8.0**0.25
MESH_ID = pl.DeviceIdType.MESH
HALF = 1024
SIDE = 4
DEPTH = 8
CAP = 64
ROWS = 128
HALO = 32
TAPS = 31
PLACE = {1: 0, 7: 1, 2: 2, 6: 3, 3: 4, 5: 5, 4: 6, 0: 7}
GROUP = ((0, 2), (2, 4), (4, 7))


def normalize(values):
    mean = jnp.mean(values, -1, keepdims=True)
    square = jnp.mean(values * values, -1, keepdims=True)
    return (values - mean) * lax.rsqrt(square - mean * mean + EPSILON)


def layer_kernel(
    linear_h, gate_h, taps_h, channel_gain_h, w_h, residual_h, mix_gain_h, docs_h, ids_h, ways_h, gain_h,
    w_gate, w_up, w_down, s_gate, s_up, s_down, out,
    taps, channel_gain, mix_gain, docs, ids, ways, gain,
    linear, gate, residual, weight, gated, tail, tail_docs, halo, halo_docs, tap32, conv, conv_in, act,
    sums, sums_in, part, part_in2, normed, table,
    wg, wu, wd, sg, su, sd,
    near, meta, packed, relay, arrived, acc_g, acc_u, hidden, answers, relay_back, back, partial, relay_part,
    part_in, kept, shared,
    l_sem, w_sem, z_r, h_r, a_r, g_r, e_r, end_r, st_r, x_r, s1_r, m_r, d_r, rl_r, b_r, bl_r, p_r,
    z_s, h_s, a_s, g_s, e_s, st_s, x_s, s1_s, m_s, d_s, rl_s, fw_s, b_s, bl_s, bf_s, p_s,
):
    f32, bf16 = jnp.float32, jnp.bfloat16
    sp, tp = lax.axis_index("sp"), lax.axis_index("tp")
    y, x = sp // SIDE, sp % SIDE
    z, core = tp // 2, tp % 2
    other = 1 - core

    def at(dy, dx):
        return ((y + dy) % SIDE) * SIDE + (x + dx) % SIDE

    def first(o, k):
        return at(0, k) if o == 0 else at(k, 0)

    def second(o, k):
        return at(k, 0) if o == 0 else at(0, k)

    def along(dz):
        return ((z + dz) % DEPTH) * 2 + core

    def push(src, dst, ss, rs, to_sp, to_tp):
        pltpu.make_async_remote_copy(
            src_ref=src, dst_ref=dst, send_sem=ss, recv_sem=rs,
            device_id=(to_sp, to_tp), device_id_type=MESH_ID,
        ).start()

    def send(src, dst, ss, rs, to):
        push(src, dst, ss, rs, to, tp)

    def landed(dst, rs):
        pltpu.make_async_remote_copy(
            src_ref=dst, dst_ref=dst, send_sem=rs, recv_sem=rs,
            device_id=(first(0, 1), tp), device_id_type=MESH_ID,
        ).wait_recv()

    def gone(src, ss):
        pltpu.make_async_remote_copy(
            src_ref=src, dst_ref=src, send_sem=ss, recv_sem=ss,
            device_id=(first(0, 1), tp), device_id_type=MESH_ID,
        ).wait_send()

    own_loads = [
        pltpu.make_async_copy(a, b, l_sem.at[i])
        for i, (a, b) in enumerate(
            [
                (w_h, weight.at[7]), (linear_h, linear), (gate_h, gate), (docs_h, docs), (ids_h, ids),
                (ways_h, ways), (taps_h, taps), (channel_gain_h, channel_gain), (mix_gain_h, mix_gain),
                (gain_h, gain), (residual_h, residual),
            ]
        )
    ]
    for load in own_loads:
        load.start()
    loads = [
        pltpu.make_async_copy(a, b, w_sem.at[i])
        for i, (a, b) in enumerate(
            [(s_gate, sg), (s_up, su), (s_down, sd), (w_gate, wg), (w_up, wu), (w_down, wd)]
        )
    ]

    after, ahead = (sp + 1) % 16, (sp + 15) % 16
    barrier = pltpu.get_barrier_semaphore()

    def greet(to_sp, to_tp):
        pl.semaphore_signal(barrier, inc=1, device_id=(to_sp, to_tp), device_id_type=MESH_ID)

    for dz in (1, 7):
        greet(sp, along(dz))
    for to in (at(0, 1), at(0, 3), at(1, 0), at(3, 0), after, ahead):
        greet(to, tp)
    greet(sp, z * 2 + other)
    pl.semaphore_wait(barrier, 9)

    def columns(o, k, ks=0):
        fast, slow = (x, y) if o == 0 else (y, x)
        block = ((slow + ks) % SIDE) * SIDE + (fast + k) % SIDE
        return pl.ds(pl.multiple_of(block * 128, 128), 128)

    def strip(o):
        return slice(o * 64, o * 64 + 64)

    def upper(o):
        return slice(o * 64, o * 64 + 32)

    def lower(o):
        return slice(o * 64 + 32, o * 64 + 64)

    def hop(here, there, dz):
        for o in (0, 1):
            push(
                weight.at[here, strip(o), columns(o, 0)], weight.at[there, strip(o), columns(o, 0)],
                z_s, z_r.at[there], sp, along(dz),
            )

    def hopped(there):
        landed(weight.at[there, :, 0:128], z_r.at[there])

    own_loads[0].wait()
    hop(7, PLACE[7], 1)
    hop(7, PLACE[1], 7)

    for load in own_loads[1:4]:
        load.wait()

    def gate_rows(a, b):
        a, b = a.astype(f32), b.astype(f32)
        return (a * (1.0 / (1.0 + jnp.exp(-b)))).astype(bf16)

    tail[...] = gate_rows(linear[2048 - HALO:, :], gate[2048 - HALO:, :])
    doc = docs[...]
    spot = lax.broadcasted_iota(jnp.int32, (16, 128), 0) * 128 + lax.broadcasted_iota(jnp.int32, (16, 128), 1)
    local, last = [], []
    for d in (1, 2, 3):
        below = jnp.where(doc < d, 1.0, 0.0)
        local.append(jnp.sum(jnp.sum(below, 1, keepdims=True), 0, keepdims=True))
        below = jnp.where(spot >= 2048 - (TAPS - 1), below, 0.0)
        last.append(jnp.sum(jnp.sum(below, 1, keepdims=True), 0, keepdims=True))
    for i in range(3):
        tail_docs[i:i + 1, :] = jnp.broadcast_to(last[i], (1, 128))
    tail_docs[3:8, :] = jnp.zeros((5, 128), f32)
    push(tail, halo, h_s.at[0], h_r.at[0], after, tp)
    push(tail_docs, halo_docs, h_s.at[1], h_r.at[1], after, tp)
    for load in loads:
        load.start()

    def gate_block(i, _):
        rows = pl.ds(pl.multiple_of(i * 128, 128), 128)
        there = pl.ds(pl.multiple_of(i * 128 + HALO, 32), 128)
        gated[there, :] = gate_rows(linear[rows, :], gate[rows, :]).astype(f32)
        return 0

    lax.fori_loop(0, 16, gate_block, 0)
    for load in own_loads[4:10]:
        load.wait()
    tap32[0:TAPS, :] = taps[...].astype(f32)

    def spread(o, g, k):
        lo, hi = GROUP[g]
        mine = weight.at[lo:hi, strip(o), columns(o, k)]
        late = 1 if k == 2 else 0
        send(mine, mine, e_s, e_r.at[o, g, late, 0], second(o, 1))
        send(mine, mine, e_s, e_r.at[o, g, late, 1], second(o, 3))

    def gather_start(g):
        lo, hi = GROUP[g]
        for o in (0, 1):
            mine = weight.at[lo:hi, strip(o), columns(o, 0)]
            send(mine, mine, g_s, g_r.at[o, g, 0], first(o, 1))
            send(mine, mine, g_s, g_r.at[o, g, 1], first(o, 3))
        for o in (0, 1):
            spread(o, g, 0)

    def gather_near(g):
        lo, hi = GROUP[g]
        for o in (0, 1):
            landed(weight.at[lo:hi, strip(o), columns(o, 3)], g_r.at[o, g, 0])
            half = weight.at[lo:hi, upper(o), columns(o, 3)]
            send(half, half, g_s, g_r.at[o, g, 2], first(o, 1))
            landed(weight.at[lo:hi, strip(o), columns(o, 1)], g_r.at[o, g, 1])
            half = weight.at[lo:hi, lower(o), columns(o, 1)]
            send(half, half, g_s, g_r.at[o, g, 2], first(o, 3))
        for o in (0, 1):
            spread(o, g, 3)
            spread(o, g, 1)

    def gather_far(g):
        lo, hi = GROUP[g]
        for o in (0, 1):
            landed(weight.at[lo:hi, strip(o), columns(o, 2)], g_r.at[o, g, 2])
            spread(o, g, 2)

    def gather_pass(g, ks):
        lo, hi = GROUP[g]
        late = 1 if ks == (2,) else 0
        for o in (0, 1):
            landed(weight.at[lo:hi, strip(o), 0:128 * len(ks)], e_r.at[o, g, late, 0])
            for k in ks:
                half = weight.at[lo:hi, upper(o), columns(o, k, 3)]
                send(half, half, e_s, end_r.at[o, g], second(o, 1))
            landed(weight.at[lo:hi, strip(o), 0:128 * len(ks)], e_r.at[o, g, late, 1])
            for k in ks:
                half = weight.at[lo:hi, lower(o), columns(o, k, 1)]
                send(half, half, e_s, end_r.at[o, g], second(o, 3))

    def gather_end(g):
        lo, hi = GROUP[g]
        for o in (0, 1):
            landed(weight.at[lo:hi, strip(o), 0:512], end_r.at[o, g])

    SOON = (0, 3, 1)

    names = lax.broadcasted_iota(jnp.int32, (16, ROWS), 0)
    hit_0, hit_1 = names == ids[0:1, :], names == ids[1:2, :]
    hits = jnp.where(hit_0 | hit_1, 1.0, 0.0)
    before = lax.broadcasted_iota(jnp.int32, (ROWS, ROWS), 0) < lax.broadcasted_iota(jnp.int32, (ROWS, ROWS), 1)
    ranks = jnp.dot(hits.astype(bf16), jnp.where(before, 1.0, 0.0).astype(bf16), preferred_element_type=f32)
    slots = jnp.where(hits > 0.5, ranks, -1.0)
    values = jnp.where(hit_0, ways[0:1, :], 0.0) + jnp.where(hit_1, ways[1:2, :], 0.0)
    for e in range(16):
        table[e] = slots[e:e + 1, :]
        table[e + 16] = values[e:e + 1, :]

    hopped(PLACE[7])
    hop(PLACE[7], PLACE[6], 1)
    hopped(PLACE[1])
    hop(PLACE[1], PLACE[2], 7)
    gather_start(0)
    landed(halo, h_r.at[0])
    landed(halo_docs, h_r.at[1])
    inside = sp > 0
    gated[0:HALO, :] = jnp.where(inside, halo[...].astype(f32), 0.0)
    starts = []
    for i in range(3):
        extra = jnp.where(inside, halo_docs[i:i + 1, :], float(TAPS - 1)) - float(TAPS - 1)
        starts.append(local[i] + extra)

    CHUNK = 64

    def conv_block(dz):
        base = ((z + dz) % DEPTH) * 256

        def piece(i, _):
            row = pl.multiple_of(base + i * CHUNK, CHUNK)
            spot = lax.broadcasted_iota(jnp.int32, (CHUNK, 128), 0).astype(f32) + row.astype(f32)
            begun = jnp.full((CHUNK, 128), -1000.0, f32)
            for s in starts:
                begun = jnp.maximum(begun, jnp.where(s <= spot, s, -1000.0))
            age = spot - begun
            total = jnp.zeros((CHUNK, 128), f32)
            for j in range(TAPS):
                window = gated[pl.ds(row + (HALO - j), CHUNK), :]
                total = total + jnp.where(age >= float(j), window * tap32[j:j + 1, :], 0.0)
            conv[pl.ds(row, CHUNK), :] = total.astype(bf16)
            return 0

        lax.fori_loop(0, 256 // CHUNK, piece, 0)
        rows = pl.ds(pl.multiple_of(base, 256), 256)
        if dz == 0:
            conv_in[:, 7 * 128:] = conv[rows, :]
        else:
            there = PLACE[(DEPTH - dz) % DEPTH]
            push(
                conv.at[rows, :], conv_in.at[:, there * 128:(there + 1) * 128],
                a_s, a_r, sp, along(dz),
            )

    conv_block(1)
    conv_block(7)
    hopped(PLACE[6])
    hop(PLACE[6], PLACE[5], 1)
    hopped(PLACE[2])
    hop(PLACE[2], PLACE[3], 7)
    gather_start(1)
    conv_block(2)
    gather_near(0)
    conv_block(6)
    hopped(PLACE[5])
    hop(PLACE[5], PLACE[4], 1)
    hopped(PLACE[3])
    conv_block(3)
    conv_block(5)
    gather_far(0)
    gather_near(1)
    hopped(PLACE[4])
    gather_start(2)
    conv_block(4)
    conv_block(0)
    gather_far(1)
    gather_pass(0, SOON)
    gather_near(2)
    gather_pass(0, (2,))
    gather_far(2)
    gather_pass(1, SOON)
    gather_pass(1, (2,))

    landed(conv_in.at[:, 0:7 * 128], a_r)
    mean_part = jnp.zeros((256, 128), f32)
    square_part = jnp.zeros((256, 128), f32)
    for s in range(DEPTH):
        v = conv_in[:, s * 128:(s + 1) * 128].astype(f32)
        mean_part = mean_part + v
        square_part = square_part + v * v
    sums[0] = mean_part
    sums[1] = square_part
    push(sums, sums_in, st_s, st_r, sp, z * 2 + other)
    gather_pass(2, SOON)
    gather_pass(2, (2,))
    landed(sums_in, st_r)
    mean = jnp.sum(sums[0] + sums_in[0], 1, keepdims=True) * (1.0 / 2048.0)
    square = jnp.sum(sums[1] + sums_in[1], 1, keepdims=True) * (1.0 / 2048.0)
    scale = lax.rsqrt(square - mean * mean + EPSILON)
    for dz, s in PLACE.items():
        v = conv_in[:, s * 128:(s + 1) * 128].astype(f32)
        v = (v - mean) * scale * channel_gain[along(dz)]
        act[:, s * 128:(s + 1) * 128] = (v / (1.0 + jnp.exp(-v))).astype(bf16)

    for g, (lo, hi) in enumerate(((0, 2), (2, 4), (4, 8))):
        gather_end(g)
        for n in range(4):
            w = weight[lo:hi, :, n * 512:(n + 1) * 512].reshape((hi - lo) * 128, 512)
            got = jnp.dot(act[:, lo * 128:hi * 128], w, preferred_element_type=f32).reshape(2, ROWS, 512)
            part[n] = got if g == 0 else part[n] + got
            if g == 2:
                push(part.at[n, other], part_in2.at[n], x_s, x_r.at[n], sp, z * 2 + other)
    own_loads[10].wait()
    for n in range(4):
        cols = slice(n * 512, (n + 1) * 512)
        landed(part_in2.at[n], x_r.at[n])
        kept[:, cols] = RESIDUAL_SCALE * residual[:, cols].astype(f32) + part[n, core] + part_in2[n]
    normed[...] = (normalize(kept[...]) * mix_gain[...]).astype(bf16)

    for o in (0, 1):
        mine = normed.at[:, o * HALF:(o + 1) * HALF]
        send(table, meta.at[o, 3], m_s, m_r.at[o, 0], first(o, 1))
        send(table, meta.at[o, 1], m_s, m_r.at[o, 1], first(o, 3))
        send(mine, near.at[o, 3], s1_s, s1_r.at[o, 0], first(o, 1))
        send(mine, near.at[o, 1], s1_s, s1_r.at[o, 1], first(o, 3))

    lanes = lax.broadcasted_iota(jnp.int32, (CAP, 128), 0).astype(f32)

    def expert_at(o, k):
        return second(o, k)

    def slot_row(o, k, e):
        return table[e] if k == 0 else meta[o, k, e]

    def weight_row(o, k, e):
        return table[e + 16] if k == 0 else meta[o, k, e + 16]

    def pack(o, k):
        rows = normed[:, o * HALF:(o + 1) * HALF] if k == 0 else near[o, k]
        for q in (2, 1, 3, 0):
            hit = jnp.where(lanes == slot_row(o, k, expert_at(o, q)), 1.0, 0.0).astype(bf16)
            block = jnp.dot(hit, rows, preferred_element_type=f32).astype(bf16)
            if q == 0:
                arrived[o, 0, k] = block
            else:
                packed[o, q - 1, k] = block
            if q == 2:
                way = 1 if k < 2 else 3
                send(packed.at[o, 1, k], relay.at[o, k], rl_s, rl_r.at[o, k], second(o, way))
            if q == 1:
                send(packed.at[o, 0, k], arrived.at[o, 3, k], d_s, d_r.at[o, k], second(o, 1))
            if q == 3:
                send(packed.at[o, 2, k], arrived.at[o, 1, k], d_s, d_r.at[o, k], second(o, 3))

    def pass_on(o, k):
        landed(relay.at[o, k], rl_r.at[o, k])
        way = 1 if k < 2 else 3
        send(relay.at[o, k], arrived.at[o, 2, k], fw_s, d_r.at[o, k], second(o, way))

    for o in (0, 1):
        pack(o, 0)
    gone(weight.at[0:7, :, 0:128], z_s)
    gone(tail, h_s.at[0])
    gone(tail_docs, h_s.at[1])
    gone(conv_in.at[:, 0:7 * 128], a_s)
    gone(weight.at[0:7, :, 0:384], g_s)
    gone(weight.at[0:7, :, 0:1536], e_s)
    gone(sums, st_s)
    gone(part_in2, x_s)
    for o in (0, 1):
        landed(meta.at[o, 3], m_r.at[o, 0])
        send(meta.at[o, 3], meta.at[o, 2], m_s, m_r.at[o, 2], first(o, 1))
        landed(near.at[o, 3], s1_r.at[o, 0])
        send(near.at[o, 3, 0:64], near.at[o, 2, 0:64], s1_s, s1_r.at[o, 2], first(o, 1))
    for o in (0, 1):
        landed(meta.at[o, 1], m_r.at[o, 1])
        landed(near.at[o, 1], s1_r.at[o, 1])
        send(near.at[o, 1, 64:128], near.at[o, 2, 64:128], s1_s, s1_r.at[o, 2], first(o, 3))
    for k in (3, 1):
        for o in (0, 1):
            pack(o, k)
    for o in (0, 1):
        pass_on(o, 0)
    for o in (0, 1):
        landed(meta.at[o, 2], m_r.at[o, 2])
        landed(near.at[o, 2], s1_r.at[o, 2])
        pack(o, 2)

    acc_g[...] = jnp.zeros_like(acc_g)
    acc_u[...] = jnp.zeros_like(acc_u)
    for load in loads[:3]:
        load.wait()
    act = jnp.dot(normed[...], sg[...], preferred_element_type=f32)
    lin = jnp.dot(normed[...], su[...], preferred_element_type=f32)
    common = (act / (1.0 + jnp.exp(-act)) * lin).astype(bf16)
    shared[...] = jnp.dot(common, sd[...], preferred_element_type=f32)
    for k in (3, 1):
        for o in (0, 1):
            pass_on(o, k)
    for load in loads[3:]:
        load.wait()

    def product(o, k):
        landed(arrived.at[o, 1:4, k], d_r.at[o, k])
        rows = arrived[o, :, k].reshape(SIDE * CAP, HALF)
        for acc, w in ((acc_g, wg), (acc_u, wu)):
            got = jnp.dot(rows, w[o * HALF:(o + 1) * HALF, :], preferred_element_type=f32)
            got = got.reshape(SIDE, CAP, 512)
            if o == 0:
                acc[:, k] = acc[:, k] + got
            else:
                acc[k] = acc[k] + got

    for o in (0, 1):
        product(o, 0)
    for o in (0, 1):
        pass_on(o, 2)
    for k in (3, 1, 2):
        for o in (0, 1):
            product(o, k)

    def relayed(k):
        for o in (0, 1):
            way = 1 if k < 2 else 3
            send(answers.at[o, 1, k], relay_back.at[o, k], bl_s, bl_r.at[o, k], second(o, way))

    def direct(k):
        for o in (0, 1):
            for q in (1, 3):
                send(answers.at[o, q - 1, k], back.at[o, k, SIDE - q], b_s, b_r.at[o, k], second(o, q))

    def pass_back(o, k):
        landed(relay_back.at[o, k], bl_r.at[o, k])
        way = 1 if k < 2 else 3
        send(relay_back.at[o, k], back.at[o, k, 2], bf_s, b_r.at[o, k], second(o, way))

    ready = set()

    def hide(dy, dx):
        if (dy, dx) not in ready:
            ready.add((dy, dx))
            g = acc_g[dy, dx]
            hidden[dy, dx] = (g / (1.0 + jnp.exp(-g)) * acc_u[dy, dx]).astype(bf16)

    def answer(k):
        for o in (0, 1):
            for q in range(SIDE):
                hide(*((q, k) if o == 0 else (k, q)))
            rows = (hidden[:, k] if o == 0 else hidden[k]).reshape(SIDE * CAP, 512)
            ans = jnp.dot(rows, wd[:, o * HALF:(o + 1) * HALF], preferred_element_type=f32).astype(bf16)
            back[o, k, 0] = ans[0:CAP]
            for q in (1, 2, 3):
                answers[o, q - 1, k] = ans[q * CAP:(q + 1) * CAP]

    answer(2)
    relayed(2)
    direct(2)
    answer(1)
    relayed(1)
    answer(3)
    relayed(3)
    answer(0)

    def choose(o, k, part):
        rows = []
        for j in range(SIDE):
            e = expert_at(o, j)
            w = weight_row(o, k, e)
            high = w.astype(bf16).astype(f32)
            value = high if part == 0 else w - high
            rows.append(jnp.where(lanes == slot_row(o, k, e), value, 0.0).astype(bf16))
        return jnp.concatenate(rows, 0)

    def combine(o, k):
        landed(back.at[o, k, 1:4], b_r.at[o, k])
        rows = back[o, k].reshape(SIDE * CAP, HALF)
        dims = (((0,), (0,)), ((), ()))
        total = lax.dot_general(choose(o, k, 0), rows, dims, preferred_element_type=f32)
        return total + lax.dot_general(choose(o, k, 1), rows, dims, preferred_element_type=f32)

    def pass_sum(o, k):
        total = combine(o, k)
        mine = partial.at[o, k - 1]
        if k == 2:
            partial[o, k - 1] = total.astype(bf16)
            send(mine.at[0:64], relay_part.at[o, 0], p_s, p_r.at[o, 0], first(o, 1))
            send(mine.at[64:128], relay_part.at[o, 1], p_s, p_r.at[o, 1], first(o, 3))
        elif k == 1:
            landed(relay_part.at[o, 0], p_r.at[o, 0])
            partial[o, k - 1, 0:64] = (total[0:64] + relay_part[o, 0].astype(f32)).astype(bf16)
            partial[o, k - 1, 64:128] = total[64:128].astype(bf16)
            send(mine, part_in.at[o, 0], p_s, p_r.at[o, 2], first(o, 1))
        else:
            landed(relay_part.at[o, 1], p_r.at[o, 1])
            partial[o, k - 1, 0:64] = total[0:64].astype(bf16)
            partial[o, k - 1, 64:128] = (total[64:128] + relay_part[o, 1].astype(f32)).astype(bf16)
            send(mine, part_in.at[o, 1], p_s, p_r.at[o, 2], first(o, 3))

    def both(step, k):
        for o in (0, 1):
            step(o, k)

    both(pass_back, 2)
    direct(1)
    both(pass_back, 1)
    direct(3)
    both(pass_back, 3)
    relayed(0)
    gone(meta.at[:, 0:3], m_s)
    gone(near.at[:, 0:3], s1_s)
    gone(arrived.at[0], d_s)
    gone(relay, rl_s)
    gone(relay, fw_s)
    both(pass_sum, 2)
    direct(0)
    both(pass_back, 0)
    both(pass_sum, 1)
    both(pass_sum, 3)
    for o in (0, 1):
        kept[:, o * HALF:(o + 1) * HALF] = combine(o, 0)
    gone(back.at[0], b_s)
    gone(relay_back, bl_s)
    gone(relay_back, bf_s)
    for o in (0, 1):
        landed(part_in.at[o], p_r.at[o, 2])
        here = slice(o * HALF, (o + 1) * HALF)
        kept[:, here] = kept[:, here] + part_in[o, 0].astype(f32) + part_in[o, 1].astype(f32)
    values = RESIDUAL_SCALE * normed[...].astype(f32) + kept[...] + shared[...]
    out[...] = (normalize(values) * gain[...]).astype(bf16)
    gone(near.at[:, 0:3], p_s)


def shards(
    linear_part, gate_part, kernel_taps, channel_gain, output_weight, residual, mix_gain, documents,
    expert_ids, route_weights, expert_gate, expert_up, expert_down, shared_gate, shared_up, shared_down,
    final_gain,
):
    bf16, f32 = jnp.bfloat16, jnp.float32
    dma = pltpu.SemaphoreType.DMA
    vmem = pl.BlockSpec(memory_space=pltpu.VMEM)
    hbm = pl.BlockSpec(memory_space=pltpu.MemorySpace.HBM)
    block = (CAP, HALF)
    w_gate, w_up, w_down = expert_gate[0], expert_up[0], expert_down[0]
    args = (
        (linear_part, hbm), (gate_part, hbm), (kernel_taps, hbm), (channel_gain.reshape(16, 1, 128), hbm),
        (output_weight, hbm), (residual, hbm), (mix_gain[None, :], hbm), (documents.reshape(16, 128), hbm),
        (expert_ids.T, hbm), (route_weights.T, hbm), (final_gain[None, :], hbm),
        (w_gate, hbm), (w_up, hbm), (w_down, hbm), (shared_gate, hbm), (shared_up, hbm), (shared_down, hbm),
    )
    return pl.pallas_call(
        layer_kernel,
        out_shape=jax.ShapeDtypeStruct(residual.shape, bf16),
        in_specs=[spec for _, spec in args],
        out_specs=vmem,
        scratch_shapes=[
            pltpu.VMEM((TAPS, 128), bf16),
            pltpu.VMEM((16, 1, 128), f32),
            pltpu.VMEM((1, 2048), f32),
            pltpu.VMEM((16, 128), jnp.int32),
            pltpu.VMEM((2, ROWS), jnp.int32),
            pltpu.VMEM((2, ROWS), f32),
            pltpu.VMEM((1, 2048), f32),
            pltpu.VMEM((2048, 128), bf16),
            pltpu.VMEM((2048, 128), bf16),
            pltpu.VMEM((ROWS, 2048), bf16),
            pltpu.VMEM((DEPTH, 128, 2048), bf16),
            pltpu.VMEM((2048 + HALO, 128), f32),
            pltpu.VMEM((HALO, 128), bf16),
            pltpu.VMEM((8, 128), f32),
            pltpu.VMEM((HALO, 128), bf16),
            pltpu.VMEM((8, 128), f32),
            pltpu.VMEM((32, 128), f32),
            pltpu.VMEM((2048, 128), bf16),
            pltpu.VMEM((256, HALF), bf16),
            pltpu.VMEM((256, HALF), bf16),
            pltpu.VMEM((2, 256, 128), f32),
            pltpu.VMEM((2, 256, 128), f32),
            pltpu.VMEM((4, 2, ROWS, 512), f32),
            pltpu.VMEM((4, ROWS, 512), f32),
            pltpu.VMEM((ROWS, 2048), bf16),
            pltpu.VMEM((32, 1, 128), f32),
            pltpu.VMEM(w_gate.shape, bf16),
            pltpu.VMEM(w_up.shape, bf16),
            pltpu.VMEM(w_down.shape, bf16),
            pltpu.VMEM(shared_gate.shape, bf16),
            pltpu.VMEM(shared_up.shape, bf16),
            pltpu.VMEM(shared_down.shape, bf16),
            pltpu.VMEM((2, 4, ROWS, HALF), bf16),
            pltpu.VMEM((2, 4, 32, 1, 128), f32),
            pltpu.VMEM((2, 3, 4) + block, bf16),
            pltpu.VMEM((2, 4) + block, bf16),
            pltpu.VMEM((2, 4, 4) + block, bf16),
            pltpu.VMEM((4, 4, CAP, 512), f32),
            pltpu.VMEM((4, 4, CAP, 512), f32),
            pltpu.VMEM((4, 4, CAP, 512), bf16),
            pltpu.VMEM((2, 3, 4) + block, bf16),
            pltpu.VMEM((2, 4) + block, bf16),
            pltpu.VMEM((2, 4, 4) + block, bf16),
            pltpu.VMEM((2, 3, ROWS, HALF), bf16),
            pltpu.VMEM((2, 2) + block, bf16),
            pltpu.VMEM((2, 2, ROWS, HALF), bf16),
            pltpu.VMEM((ROWS, 2048), f32),
            pltpu.VMEM((ROWS, 2048), f32),
            dma((11,)), dma((6,)), dma((7,)), dma((2,)), dma, dma((2, 3, 3)), dma((2, 3, 2, 2)), dma((2, 3)),
            dma, dma((4,)), dma((2, 3)), dma((2, 3)), dma((2, 4)), dma((2, 4)), dma((2, 4)), dma((2, 4)),
            dma((2, 3)),
            dma, dma((2,)), dma, dma, dma, dma, dma, dma, dma, dma, dma, dma, dma, dma, dma, dma,
        ],
        compiler_params=pltpu.CompilerParams(
            collective_id=0, has_side_effects=True, vmem_limit_bytes=54 * 1024 * 1024
        ),
    )(*[a for a, _ in args])


def solution(mesh):
    both = P(("sp", "tp"), None)
    placed = (
        P("sp", "tp"), P("sp", "tp"), P(None, "tp"), P(), P("tp", None), both, P(), P("sp"), both, both,
        P("sp", None, None), P("sp", None, None), P("sp", None, None), P(), P(), P(), P(),
    )
    return jax.shard_map(shards, mesh=mesh, in_specs=placed, out_specs=both, check_vma=False)
```

time: 123 us -> 117 us (0.951)
  Pallas kernels: 120 us -> 115 us
    pallas_call x1, Pallas kernels: 120 us -> 115 us  [shards(): pl.pallas_call(layer_kernel, out_shape=jax.ShapeDtypeStruct(residual.shap...]
where the time goes in v5:
time: 117 us
  Pallas kernels  115 us (98%)
  local copies, waits for them, and re-layouts  1.88 us (2%)
    pallas_call x1, Pallas kernels, shards(): pl.pallas_call(layer_kernel, out_shape=jax.ShapeDtypeStruct(residual.shap...  115 us

profile of v5, /device:TPU:1, one launch (start us, length us, event | category | flops | bytes accessed | tf_op | source)
XLA Modules:
  0.0 117.0 jit_solution(17098293711395457403)
XLA Ops:
  0.0 115.1 %shard_map.163 = bf16[128,2048]{1,0:T(8,128)(2,1)} custom-call(bf16[2048,128]{1,0:T(8,128)(2,1)} %linear_h.1, bf16[2048,128]{1,0:T(8,128)(2,1)} %gate_h.1, bf16[31,128]{1,0:T(8,128)(2,1)} %taps_h.1, f32[16,1,128]{2,1,0:T(1,128)} %bitcast.12, bf16[128,2048]{1,0:T(8,128)(2,1)} %w_h.1, bf16[128,2048]{1,0:T(8,128)(2,1)} %residual_h.1, f32[1,2048]{1,0:T(1,128)} %bitcast.13, ...), custom_call_target="tpu_custom_call" | custom-call | tf_op jit(solution)/shard_map/pallas_call | solution.py:579
  115.1 1.9 %copy.19 = bf16[128,2048]{1,0:T(8,128)(2,1)} copy(bf16[128,2048]{1,0:T(8,128)(2,1)} %shard_map.163) | data formatting | bytes 1048576

commit v6 on v5

--- a/solution.py
+++ b/solution.py
@@ -101,12 +101,12 @@
     def greet(to_sp, to_tp):
         pl.semaphore_signal(barrier, inc=1, device_id=(to_sp, to_tp), device_id_type=MESH_ID)
 
-    for dz in (1, 7):
+    for dz in (1, 7, 2, 6):
         greet(sp, along(dz))
     for to in (at(0, 1), at(0, 3), at(1, 0), at(3, 0), after, ahead):
         greet(to, tp)
     greet(sp, z * 2 + other)
-    pl.semaphore_wait(barrier, 9)
+    pl.semaphore_wait(barrier, 11)
 
     def columns(o, k, ks=0):
         fast, slow = (x, y) if o == 0 else (y, x)
@@ -135,6 +135,8 @@
     own_loads[0].wait()
     hop(7, PLACE[7], 1)
     hop(7, PLACE[1], 7)
+    hop(7, PLACE[6], 2)
+    hop(7, PLACE[2], 6)
 
     for load in own_loads[1:4]:
         load.wait()
@@ -174,7 +176,7 @@
     def spread(o, g, k):
         lo, hi = GROUP[g]
         mine = weight.at[lo:hi, strip(o), columns(o, k)]
-        late = 1 if k == 2 else 0
+        late = (0, 1, 2, 1)[k]
         send(mine, mine, e_s, e_r.at[o, g, late, 0], second(o, 1))
         send(mine, mine, e_s, e_r.at[o, g, late, 1], second(o, 3))
 
@@ -208,7 +210,7 @@
 
     def gather_pass(g, ks):
         lo, hi = GROUP[g]
-        late = 1 if ks == (2,) else 0
+        late = (0, 1, 2, 1)[ks[0]]
         for o in (0, 1):
             landed(weight.at[lo:hi, strip(o), 0:128 * len(ks)], e_r.at[o, g, late, 0])
             for k in ks:
@@ -224,7 +226,7 @@
         for o in (0, 1):
             landed(weight.at[lo:hi, strip(o), 0:512], end_r.at[o, g])
 
-    SOON = (0, 3, 1)
+    OWN, SIDES, FAR = (0,), (3, 1), (2,)
 
     names = lax.broadcasted_iota(jnp.int32, (16, ROWS), 0)
     hit_0, hit_1 = names == ids[0:1, :], names == ids[1:2, :]
@@ -236,12 +238,19 @@
     for e in range(16):
         table[e] = slots[e:e + 1, :]
         table[e + 16] = values[e:e + 1, :]
+    for o in (0, 1):
+        send(table, meta.at[o, 3], m_s, m_r.at[o, 0], first(o, 1))
+        send(table, meta.at[o, 1], m_s, m_r.at[o, 1], first(o, 3))
 
     hopped(PLACE[7])
-    hop(PLACE[7], PLACE[6], 1)
     hopped(PLACE[1])
-    hop(PLACE[1], PLACE[2], 7)
     gather_start(0)
+    hopped(PLACE[6])
+    hop(PLACE[6], PLACE[5], 1)
+    hop(PLACE[6], PLACE[4], 2)
+    hopped(PLACE[2])
+    hop(PLACE[2], PLACE[3], 7)
+    gather_start(1)
     landed(halo, h_r.at[0])
     landed(halo_docs, h_r.at[1])
     inside = sp > 0
@@ -274,7 +283,10 @@
         rows = pl.ds(pl.multiple_of(base, 256), 256)
         if dz == 0:
             conv_in[:, 7 * 128:] = conv[rows, :]
-        else:
+
+    def conv_send(*steps):
+        for dz in steps:
+            rows = pl.ds(pl.multiple_of(((z + dz) % DEPTH) * 256, 256), 256)
             there = PLACE[(DEPTH - dz) % DEPTH]
             push(
                 conv.at[rows, :], conv_in.at[:, there * 128:(there + 1) * 128],
@@ -283,32 +295,39 @@
 
     conv_block(1)
     conv_block(7)
-    hopped(PLACE[6])
-    hop(PLACE[6], PLACE[5], 1)
-    hopped(PLACE[2])
-    hop(PLACE[2], PLACE[3], 7)
-    gather_start(1)
+    for o in (0, 1):
+        landed(meta.at[o, 3], m_r.at[o, 0])
+        send(meta.at[o, 3], meta.at[o, 2], m_s, m_r.at[o, 2], first(o, 1))
+        landed(meta.at[o, 1], m_r.at[o, 1])
+    gather_near(0)
     conv_block(2)
-    gather_near(0)
-    conv_block(6)
+    gather_pass(0, OWN)
     hopped(PLACE[5])
-    hop(PLACE[5], PLACE[4], 1)
     hopped(PLACE[3])
-    conv_block(3)
-    conv_block(5)
-    gather_far(0)
-    gather_near(1)
     hopped(PLACE[4])
     gather_start(2)
+    conv_send(2, 1, 7)
+    conv_block(6)
+    conv_send(6)
+    gather_near(1)
+    gather_far(0)
+    conv_block(3)
+    conv_send(3)
+    gather_pass(0, SIDES)
+    gather_pass(1, OWN)
+    conv_block(5)
+    conv_send(5)
+    gather_near(2)
     conv_block(4)
+    conv_send(4)
+    gather_far(1)
     conv_block(0)
-    gather_far(1)
-    gather_pass(0, SOON)
-    gather_near(2)
-    gather_pass(0, (2,))
+    gather_pass(1, SIDES)
+    gather_pass(0, FAR)
+    gather_pass(2, OWN)
     gather_far(2)
-    gather_pass(1, SOON)
-    gather_pass(1, (2,))
+    gather_pass(1, FAR)
+    gather_pass(2, SIDES)
 
     landed(conv_in.at[:, 0:7 * 128], a_r)
     mean_part = jnp.zeros((256, 128), f32)
@@ -320,8 +339,7 @@
     sums[0] = mean_part
     sums[1] = square_part
     push(sums, sums_in, st_s, st_r, sp, z * 2 + other)
-    gather_pass(2, SOON)
-    gather_pass(2, (2,))
+    gather_pass(2, FAR)
     landed(sums_in, st_r)
     mean = jnp.sum(sums[0] + sums_in[0], 1, keepdims=True) * (1.0 / 2048.0)
     square = jnp.sum(sums[1] + sums_in[1], 1, keepdims=True) * (1.0 / 2048.0)
@@ -330,6 +348,9 @@
         v = conv_in[:, s * 128:(s + 1) * 128].astype(f32)
         v = (v - mean) * scale * channel_gain[along(dz)]
         act[:, s * 128:(s + 1) * 128] = (v / (1.0 + jnp.exp(-v))).astype(bf16)
+
+    for o in (0, 1):
+        landed(meta.at[o, 2], m_r.at[o, 2])
 
     for g, (lo, hi) in enumerate(((0, 2), (2, 4), (4, 8))):
         gather_end(g)
@@ -348,8 +369,6 @@
 
     for o in (0, 1):
         mine = normed.at[:, o * HALF:(o + 1) * HALF]
-        send(table, meta.at[o, 3], m_s, m_r.at[o, 0], first(o, 1))
-        send(table, meta.at[o, 1], m_s, m_r.at[o, 1], first(o, 3))
         send(mine, near.at[o, 3], s1_s, s1_r.at[o, 0], first(o, 1))
         send(mine, near.at[o, 1], s1_s, s1_r.at[o, 1], first(o, 3))
 
@@ -376,10 +395,12 @@
             if q == 2:
                 way = 1 if k < 2 else 3
                 send(packed.at[o, 1, k], relay.at[o, k], rl_s, rl_r.at[o, k], second(o, way))
-            if q == 1:
-                send(packed.at[o, 0, k], arrived.at[o, 3, k], d_s, d_r.at[o, k], second(o, 1))
-            if q == 3:
-                send(packed.at[o, 2, k], arrived.at[o, 1, k], d_s, d_r.at[o, k], second(o, 3))
+        if k != 2:
+            pack_send(o, k)
+
+    def pack_send(o, k):
+        send(packed.at[o, 0, k], arrived.at[o, 3, k], d_s, d_r.at[o, k], second(o, 1))
+        send(packed.at[o, 2, k], arrived.at[o, 1, k], d_s, d_r.at[o, k], second(o, 3))
 
     def pass_on(o, k):
         landed(relay.at[o, k], rl_r.at[o, k])
@@ -397,12 +418,9 @@
     gone(sums, st_s)
     gone(part_in2, x_s)
     for o in (0, 1):
-        landed(meta.at[o, 3], m_r.at[o, 0])
-        send(meta.at[o, 3], meta.at[o, 2], m_s, m_r.at[o, 2], first(o, 1))
         landed(near.at[o, 3], s1_r.at[o, 0])
         send(near.at[o, 3, 0:64], near.at[o, 2, 0:64], s1_s, s1_r.at[o, 2], first(o, 1))
     for o in (0, 1):
-        landed(meta.at[o, 1], m_r.at[o, 1])
         landed(near.at[o, 1], s1_r.at[o, 1])
         send(near.at[o, 1, 64:128], near.at[o, 2, 64:128], s1_s, s1_r.at[o, 2], first(o, 3))
     for k in (3, 1):
@@ -411,7 +429,6 @@
     for o in (0, 1):
         pass_on(o, 0)
     for o in (0, 1):
-        landed(meta.at[o, 2], m_r.at[o, 2])
         landed(near.at[o, 2], s1_r.at[o, 2])
         pack(o, 2)
 
@@ -426,6 +443,10 @@
     for k in (3, 1):
         for o in (0, 1):
             pass_on(o, k)
+    for o in (0, 1):
+        pack_send(o, 2)
+    for o in (0, 1):
+        pass_on(o, 2)
     for load in loads[3:]:
         load.wait()
 
@@ -440,11 +461,7 @@
             else:
                 acc[k] = acc[k] + got
 
-    for o in (0, 1):
-        product(o, 0)
-    for o in (0, 1):
-        pass_on(o, 2)
-    for k in (3, 1, 2):
+    for k in (0, 3, 1, 2):
         for o in (0, 1):
             product(o, k)
 
@@ -578,7 +595,7 @@
     )
     return pl.pallas_call(
         layer_kernel,
-        out_shape=jax.ShapeDtypeStruct(residual.shape, bf16),
+        out_shape=pltpu.MemorySpace.VMEM(residual.shape, bf16),
         in_specs=[spec for _, spec in args],
         out_specs=vmem,
         scratch_shapes=[
@@ -630,7 +647,7 @@
             pltpu.VMEM((2, 2, ROWS, HALF), bf16),
             pltpu.VMEM((ROWS, 2048), f32),
             pltpu.VMEM((ROWS, 2048), f32),
-            dma((11,)), dma((6,)), dma((7,)), dma((2,)), dma, dma((2, 3, 3)), dma((2, 3, 2, 2)), dma((2, 3)),
+            dma((11,)), dma((6,)), dma((7,)), dma((2,)), dma, dma((2, 3, 3)), dma((2, 3, 3, 2)), dma((2, 3)),
             dma, dma((4,)), dma((2, 3)), dma((2, 3)), dma((2, 4)), dma((2, 4)), dma((2, 4)), dma((2, 4)),
             dma((2, 3)),
             dma, dma((2,)), dma, dma, dma, dma, dma, dma, dma, dma, dma, dma, dma, dma, dma, dma,

time: 117 us -> 111 us (0.949)
  Pallas kernels: 115 us -> 110 us
    pallas_call x1, Pallas kernels: 115 us -> 110 us  [shards(): pl.pallas_call(layer_kernel, out_shape=pltpu.MemorySpace.VMEM(residual.sh...]
where the time goes in v6:
time: 111 us
  Pallas kernels  110 us (99%)
    pallas_call x1, Pallas kernels, shards(): pl.pallas_call(layer_kernel, out_shape=pltpu.MemorySpace.VMEM(residual.sh...  110 us

profile of v6, /device:TPU:1, one launch (start us, length us, event | category | flops | bytes accessed | tf_op | source)
XLA Modules:
  0.0 110.7 jit_solution(1652486501293405461)
XLA Ops:
  0.0 109.9 %shard_map.163 = bf16[128,2048]{1,0:T(8,128)(2,1)S(1)} custom-call(bf16[2048,128]{1,0:T(8,128)(2,1)} %linear_h.1, bf16[2048,128]{1,0:T(8,128)(2,1)} %gate_h.1, bf16[31,128]{1,0:T(8,128)(2,1)} %taps_h.1, f32[16,1,128]{2,1,0:T(1,128)} %bitcast.12, bf16[128,2048]{1,0:T(8,128)(2,1)} %w_h.1, bf16[128,2048]{1,0:T(8,128)(2,1)} %residual_h.1, f32[1,2048]{1,0:T(1,128)} %bitcast.13, ...), custom_call_target="tpu_custom_call" | custom-call | tf_op jit(solution)/shard_map/pallas_call | solution.py:596
  109.9 0.8 copy.19

commit v7 on v6

--- a/solution.py
+++ b/solution.py
@@ -313,21 +313,21 @@
     gather_far(0)
     conv_block(3)
     conv_send(3)
+    gather_near(2)
     gather_pass(0, SIDES)
-    gather_pass(1, OWN)
     conv_block(5)
     conv_send(5)
-    gather_near(2)
+    gather_far(1)
+    gather_pass(1, OWN)
     conv_block(4)
     conv_send(4)
-    gather_far(1)
-    conv_block(0)
+    gather_far(2)
     gather_pass(1, SIDES)
     gather_pass(0, FAR)
+    conv_block(0)
     gather_pass(2, OWN)
-    gather_far(2)
+    gather_pass(2, SIDES)
     gather_pass(1, FAR)
-    gather_pass(2, SIDES)
 
     landed(conv_in.at[:, 0:7 * 128], a_r)
     mean_part = jnp.zeros((256, 128), f32)
@@ -461,7 +461,7 @@
             else:
                 acc[k] = acc[k] + got
 
-    for k in (0, 3, 1, 2):
+    for k in (0, 3, 1):
         for o in (0, 1):
             product(o, k)
 
@@ -470,9 +470,9 @@
             way = 1 if k < 2 else 3
             send(answers.at[o, 1, k], relay_back.at[o, k], bl_s, bl_r.at[o, k], second(o, way))
 
-    def direct(k):
-        for o in (0, 1):
-            for q in (1, 3):
+    def direct(k, ways=(1, 3)):
+        for o in (0, 1):
+            for q in ways:
                 send(answers.at[o, q - 1, k], back.at[o, k, SIDE - q], b_s, b_r.at[o, k], second(o, q))
 
     def pass_back(o, k):
@@ -488,23 +488,33 @@
             g = acc_g[dy, dx]
             hidden[dy, dx] = (g / (1.0 + jnp.exp(-g)) * acc_u[dy, dx]).astype(bf16)
 
-    def answer(k):
-        for o in (0, 1):
-            for q in range(SIDE):
-                hide(*((q, k) if o == 0 else (k, q)))
-            rows = (hidden[:, k] if o == 0 else hidden[k]).reshape(SIDE * CAP, 512)
+    def answer(k, qs=(0, 1, 2, 3)):
+        for o in (0, 1):
+            rows = []
+            for q in qs:
+                at_q = (q, k) if o == 0 else (k, q)
+                hide(*at_q)
+                rows.append(hidden[at_q])
+            rows = jnp.concatenate(rows, 0) if len(rows) > 1 else rows[0]
             ans = jnp.dot(rows, wd[:, o * HALF:(o + 1) * HALF], preferred_element_type=f32).astype(bf16)
-            back[o, k, 0] = ans[0:CAP]
-            for q in (1, 2, 3):
-                answers[o, q - 1, k] = ans[q * CAP:(q + 1) * CAP]
-
+            for i, q in enumerate(qs):
+                if q == 0:
+                    back[o, k, 0] = ans[i * CAP:(i + 1) * CAP]
+                else:
+                    answers[o, q - 1, k] = ans[i * CAP:(i + 1) * CAP]
+
+    answer(1, (0, 1, 3))
+    direct(1)
+    for o in (0, 1):
+        product(o, 2)
     answer(2)
     relayed(2)
     direct(2)
-    answer(1)
+    answer(1, (2,))
     relayed(1)
     answer(3)
     relayed(3)
+    direct(3, (1,))
     answer(0)
 
     def choose(o, k, part):
@@ -524,34 +534,40 @@
         total = lax.dot_general(choose(o, k, 0), rows, dims, preferred_element_type=f32)
         return total + lax.dot_general(choose(o, k, 1), rows, dims, preferred_element_type=f32)
 
+    def send_sum(o, k, rows):
+        place = 0 if k == 1 else 1
+        send(partial.at[o, k - 1, rows], part_in.at[o, place, rows], p_s, p_r.at[o, 2], first(o, k))
+
+    top, bottom = slice(0, 64), slice(64, 128)
+
     def pass_sum(o, k):
         total = combine(o, k)
-        mine = partial.at[o, k - 1]
         if k == 2:
-            partial[o, k - 1] = total.astype(bf16)
-            send(mine.at[0:64], relay_part.at[o, 0], p_s, p_r.at[o, 0], first(o, 1))
-            send(mine.at[64:128], relay_part.at[o, 1], p_s, p_r.at[o, 1], first(o, 3))
-        elif k == 1:
-            landed(relay_part.at[o, 0], p_r.at[o, 0])
-            partial[o, k - 1, 0:64] = (total[0:64] + relay_part[o, 0].astype(f32)).astype(bf16)
-            partial[o, k - 1, 64:128] = total[64:128].astype(bf16)
-            send(mine, part_in.at[o, 0], p_s, p_r.at[o, 2], first(o, 1))
-        else:
-            landed(relay_part.at[o, 1], p_r.at[o, 1])
-            partial[o, k - 1, 0:64] = total[0:64].astype(bf16)
-            partial[o, k - 1, 64:128] = (total[64:128] + relay_part[o, 1].astype(f32)).astype(bf16)
-            send(mine, part_in.at[o, 1], p_s, p_r.at[o, 2], first(o, 3))
+            partial[o, 1] = total.astype(bf16)
+            send(partial.at[o, 1, top], relay_part.at[o, 0], p_s, p_r.at[o, 0], first(o, 1))
+            send(partial.at[o, 1, bottom], relay_part.at[o, 1], p_s, p_r.at[o, 1], first(o, 3))
+            return
+        early, late = (bottom, top) if k == 1 else (top, bottom)
+        partial[o, k - 1, early] = total[early].astype(bf16)
+        send_sum(o, k, early)
+        kept[late, o * HALF:(o + 1) * HALF] = total[late]
+
+    def pass_rest(o, k):
+        place, late = (0, top) if k == 1 else (1, bottom)
+        landed(relay_part.at[o, place], p_r.at[o, place])
+        total = kept[late, o * HALF:(o + 1) * HALF] + relay_part[o, place].astype(f32)
+        partial[o, k - 1, late] = total.astype(bf16)
+        send_sum(o, k, late)
 
     def both(step, k):
         for o in (0, 1):
             step(o, k)
 
     both(pass_back, 2)
-    direct(1)
+    direct(3, (3,))
     both(pass_back, 1)
-    direct(3)
+    relayed(0)
     both(pass_back, 3)
-    relayed(0)
     gone(meta.at[:, 0:3], m_s)
     gone(near.at[:, 0:3], s1_s)
     gone(arrived.at[0], d_s)
@@ -559,9 +575,11 @@
     gone(relay, fw_s)
     both(pass_sum, 2)
     direct(0)
+    both(pass_sum, 1)
     both(pass_back, 0)
-    both(pass_sum, 1)
     both(pass_sum, 3)
+    both(pass_rest, 1)
+    both(pass_rest, 3)
     for o in (0, 1):
         kept[:, o * HALF:(o + 1) * HALF] = combine(o, 0)
     gone(back.at[0], b_s)

time: 111 us -> 107 us (0.964)
  Pallas kernels: 110 us -> 106 us
    pallas_call x1, Pallas kernels: 110 us -> 106 us  [shards(): pl.pallas_call(layer_kernel, out_shape=pltpu.MemorySpace.VMEM(residual.sh...]
where the time goes in v7:
time: 107 us
  Pallas kernels  106 us (99%)
    pallas_call x1, Pallas kernels, shards(): pl.pallas_call(layer_kernel, out_shape=pltpu.MemorySpace.VMEM(residual.sh...  106 us

profile of v7, /device:TPU:1, one launch (start us, length us, event | category | flops | bytes accessed | tf_op | source)
XLA Modules:
  0.0 107.1 jit_solution(4143955650636492357)
XLA Ops:
  0.0 106.3 %shard_map.163 = bf16[128,2048]{1,0:T(8,128)(2,1)S(1)} custom-call(bf16[2048,128]{1,0:T(8,128)(2,1)} %linear_h.1, bf16[2048,128]{1,0:T(8,128)(2,1)} %gate_h.1, bf16[31,128]{1,0:T(8,128)(2,1)} %taps_h.1, f32[16,1,128]{2,1,0:T(1,128)} %bitcast.12, bf16[128,2048]{1,0:T(8,128)(2,1)} %w_h.1, bf16[128,2048]{1,0:T(8,128)(2,1)} %residual_h.1, f32[1,2048]{1,0:T(1,128)} %bitcast.13, ...), custom_call_target="tpu_custom_call" | custom-call | tf_op jit(solution)/shard_map/pallas_call | solution.py:614
  106.3 0.8 copy.19

commit v8 on v7

--- a/solution.py
+++ b/solution.py
@@ -328,6 +328,7 @@
     gather_pass(2, OWN)
     gather_pass(2, SIDES)
     gather_pass(1, FAR)
+    gather_pass(2, FAR)
 
     landed(conv_in.at[:, 0:7 * 128], a_r)
     mean_part = jnp.zeros((256, 128), f32)
@@ -339,7 +340,6 @@
     sums[0] = mean_part
     sums[1] = square_part
     push(sums, sums_in, st_s, st_r, sp, z * 2 + other)
-    gather_pass(2, FAR)
     landed(sums_in, st_r)
     mean = jnp.sum(sums[0] + sums_in[0], 1, keepdims=True) * (1.0 / 2048.0)
     square = jnp.sum(sums[1] + sums_in[1], 1, keepdims=True) * (1.0 / 2048.0)

time: 107 us -> 106 us (level)
  no operation moved by 1% of the time
where the time goes in v8:
time: 106 us
  Pallas kernels  105 us (99%)
    pallas_call x1, Pallas kernels, shards(): pl.pallas_call(layer_kernel, out_shape=pltpu.MemorySpace.VMEM(residual.sh...  105 us

profile of v8, /device:TPU:1, one launch (start us, length us, event | category | flops | bytes accessed | tf_op | source)
XLA Modules:
  0.0 106.2 jit_solution(3392049348494304134)
XLA Ops:
  0.0 105.4 %shard_map.163 = bf16[128,2048]{1,0:T(8,128)(2,1)S(1)} custom-call(bf16[2048,128]{1,0:T(8,128)(2,1)} %linear_h.1, bf16[2048,128]{1,0:T(8,128)(2,1)} %gate_h.1, bf16[31,128]{1,0:T(8,128)(2,1)} %taps_h.1, f32[16,1,128]{2,1,0:T(1,128)} %bitcast.12, bf16[128,2048]{1,0:T(8,128)(2,1)} %w_h.1, bf16[128,2048]{1,0:T(8,128)(2,1)} %residual_h.1, f32[1,2048]{1,0:T(1,128)} %bitcast.13, ...), custom_call_target="tpu_custom_call" | custom-call | tf_op jit(solution)/shard_map/pallas_call | solution.py:614
  105.4 0.8 copy.19

commit v9 on v8

--- a/solution.py
+++ b/solution.py
@@ -324,11 +324,11 @@
     gather_far(2)
     gather_pass(1, SIDES)
     gather_pass(0, FAR)
-    conv_block(0)
     gather_pass(2, OWN)
     gather_pass(2, SIDES)
     gather_pass(1, FAR)
     gather_pass(2, FAR)
+    conv_block(0)
 
     landed(conv_in.at[:, 0:7 * 128], a_r)
     mean_part = jnp.zeros((256, 128), f32)

time: 106 us -> 108 us (1.019)
  Pallas kernels: 105 us -> 107 us
    pallas_call x1, Pallas kernels: 105 us -> 107 us  [shards(): pl.pallas_call(layer_kernel, out_shape=pltpu.MemorySpace.VMEM(residual.sh...]
where the time goes in v9:
time: 108 us; the launch traced here: 107 us
  Pallas kernels  107 us (99%)
    pallas_call x1, Pallas kernels, shards(): pl.pallas_call(layer_kernel, out_shape=pltpu.MemorySpace.VMEM(residual.sh...  107 us

profile of v9, /device:TPU:1, one launch (start us, length us, event | category | flops | bytes accessed | tf_op | source)
XLA Modules:
  0.0 107.5 jit_solution(1635365348050381859)
XLA Ops:
  0.0 106.7 %shard_map.163 = bf16[128,2048]{1,0:T(8,128)(2,1)S(1)} custom-call(bf16[2048,128]{1,0:T(8,128)(2,1)} %linear_h.1, bf16[2048,128]{1,0:T(8,128)(2,1)} %gate_h.1, bf16[31,128]{1,0:T(8,128)(2,1)} %taps_h.1, f32[16,1,128]{2,1,0:T(1,128)} %bitcast.12, bf16[128,2048]{1,0:T(8,128)(2,1)} %w_h.1, bf16[128,2048]{1,0:T(8,128)(2,1)} %residual_h.1, f32[1,2048]{1,0:T(1,128)} %bitcast.13, ...), custom_call_target="tpu_custom_call" | custom-call | tf_op jit(solution)/shard_map/pallas_call | solution.py:614
  106.7 0.8 copy.19
